TPU v7x, 128 devices: a whole 4x4x4 slice. The times are simulated.
128 devices in a mesh: sp: 16 (over z, y), tp: 8 (over x, core).
Axes of the slice: x: 4, y: 4, z: 4, core: 2. Of those that a mesh axis runs over, the one named last changes fastest.
Arguments:
- hidden_activations: bfloat16 [12288, 4096], P(('sp', 'tp')), may hold values from -6 to 6
- entry_rescale_vector: bfloat16 [4096], replicated, may hold values from 0.099609375 to 1.8984375
- probe_matrix: bfloat16 [4096, 2048], P('sp', 'tp'), may hold values from -0.09375 to 0.09375
- lookup_address_matrix: bfloat16 [4096, 2048], P('sp', 'tp'), may hold values from -0.09375 to 0.09375
- payload_matrix: bfloat16 [4096, 4096], P('sp', 'tp'), may hold values from -0.09375 to 0.09375
- postfilter_switch_matrix: bfloat16 [4096, 4096], P('sp', 'tp'), may hold values from -0.09375 to 0.09375
- prefilter_switch_matrix: bfloat16 [4096, 4096], P('sp', 'tp'), may hold values from -0.09375 to 0.09375
- filter_source_matrix: bfloat16 [4096, 4096], P('sp', 'tp'), may hold values from -0.09375 to 0.09375
- forget_left_factor: bfloat16 [4096, 64], replicated, may hold values from -0.09375 to 0.09375
- forget_right_factor: bfloat16 [64, 2048], P(None, 'tp'), may hold values from -0.75 to 0.75
- forget_offset_per_feature: float32 [2048], P('tp'), may hold values from -1 to 12
- forget_spike_additions: float32 [16, 12288], P('tp', 'sp'), may hold values from -3 to 0
- subspace_rescale_vector: bfloat16 [16, 256], P('tp'), may hold values from 0.099609375 to 1.8984375
- depthwise_filter_taps: bfloat16 [3, 4096], P(None, 'tp'), may hold values from -3.5 to 3.5
- mixer_result_matrix: bfloat16 [4096, 4096], P('tp'), may hold values from -0.09375 to 0.09375
- filter_result_matrix: bfloat16 [4096, 4096], P('tp'), may hold values from -0.09375 to 0.09375
Outputs:
- mixed: bfloat16 [12288, 4096], P(('sp', 'tp'))
All inputs are finite; a program needn't handle non-finite values.
Results may differ from a plain program's by a relative error of at most 0.02.
Values may be sent and summed in bfloat16 or wider, within the bound.
A program may use at most 128 MiB of HBM per device.

v0:
```python
import jax
import jax.numpy as jnp
from jax import lax
from jax.sharding import Mesh
from jax.sharding import PartitionSpec as P

BLOCK = 64
SP = ("sp_0", "sp_1")
SP_TP = ("sp_0", "sp_1", "tp")


epsilon = 1e-06
softness_scale = 16.0


def nothing_yet(shard, identity):
    return jax.tree.map(
        lambda part, zero: jnp.zeros_like(part) + jnp.asarray(zero, part.dtype), shard, identity
    )


def entering(shard, axes, combine, identity):
    before = start = nothing_yet(shard, identity)
    total = shard
    for axis in reversed(axes):
        size, index = (lax.axis_size(axis), lax.axis_index(axis))
        pieces = jax.tree.map(
            lambda part, kind: lax.all_gather(part.astype(kind), axis),
            total,
            (jnp.bfloat16, jnp.bfloat16),
        )
        inside, total = (start, start)
        for k in range(size):
            passed = k < index
            total = combine(
                total, jax.tree.map(lambda part, own: part[k].astype(own.dtype), pieces, shard)
            )
            inside = jax.tree.map(lambda new, old: jnp.where(passed, new, old), total, inside)
        before = combine(inside, before)
    return before


def shifted(value, axis, steps):
    count = lax.axis_size(axis)
    leading, last = (max(0, -steps), min(count, count - steps))
    return lax.ppermute(value, axis, [(source, source + steps) for source in range(leading, last)])


def in_one_piece(arrays, axis, dim, along):
    both = jnp.concatenate(arrays, axis=along)
    out, at, gathered = (lax.all_gather(both, axis, axis=dim, tiled=True), 0, [])
    for a in arrays:
        gathered.append(lax.slice_in_dim(out, at, at + a.shape[along], axis=along))
        at += a.shape[along]
    return tuple(gathered)


def norm_values(rows, gain):
    rows_f = rows.astype(jnp.float32)
    meansq = jnp.mean(rows_f * rows_f, axis=-1, keepdims=True)
    return rows_f * lax.rsqrt(meansq + epsilon) * gain.astype(jnp.float32)


def row_norm(gain, rows):
    return norm_values(rows, gain).astype(jnp.bfloat16)


def project_rows(normalized_input):

    def accumulate(totals, weight_rows, offset):
        return tuple(
            (
                jnp.dot(normalized_input, rows_now, preferred_element_type=jnp.float32)
                for rows_now in weight_rows
            )
        )

    return accumulate


def empty_slots(normalized_input, weight_list):
    return tuple(
        (
            jnp.zeros((normalized_input.shape[0], weight.shape[1]), jnp.float32)
            for weight in weight_list
        )
    )


def block_terms(query_rows, key_rows, value_rows, forget_log_rate):
    length_value, head_number, key_dim = query_rows.shape
    value_dim = value_rows.shape[2]
    block_count = length_value // BLOCK
    key_shape = (block_count, BLOCK, head_number, key_dim)
    query_f32 = query_rows.astype(jnp.float32).reshape(key_shape) * key_dim ** (-0.5)
    key_f32 = key_rows.astype(jnp.float32).reshape(key_shape)
    value_f32 = value_rows.astype(jnp.float32).reshape(block_count, BLOCK, head_number, value_dim)
    within = jnp.cumsum(forget_log_rate.reshape(key_shape), axis=1)
    block_end = within[:, -1]
    query_decayed = query_f32 * jnp.exp(within)
    key_inverse = key_f32 * jnp.exp(-within)
    key_tail = key_f32 * jnp.exp(block_end[:, None] - within)
    highest = lax.Precision.HIGHEST
    scores = jnp.einsum("nihd,njhd->nhij", query_decayed, key_inverse, precision=highest)
    causal = jnp.tril(jnp.ones((BLOCK, BLOCK), dtype=bool))
    scores = jnp.where(causal, scores, 0.0)
    inside = jnp.einsum("nhij,njhv->nihv", scores, value_f32, precision=highest)
    updates = jnp.einsum("njhd,njhv->nhdv", key_tail, value_f32, precision=highest)

    def advance(state, pair):
        decay_now, update_now = pair
        return (jnp.exp(decay_now)[..., None] * state + update_now, state)

    start_state = jnp.zeros((head_number, key_dim, value_dim), jnp.float32)
    final_state, state_in = lax.scan(advance, start_state, (block_end, updates))
    carried = jnp.einsum("nihd,nhdv->nihv", query_decayed, state_in, precision=highest)
    return (inside + carried, query_decayed, block_end, final_state)


def chain_combine(earlier, later):
    return (earlier[0] * later[0], later[0][..., None] * earlier[1] + later[1])


def attention_path(
    normalized_input,
    sum_values,
    forget_left_factor,
    forget_right_factor,
    forget_offset_per_feature,
    forget_spike_additions,
    subspace_rescale_vector,
):
    length_value = normalized_input.shape[0]
    head_number = subspace_rescale_vector.shape[0]
    value_dim = subspace_rescale_vector.shape[1]
    query_rows = sum_values[0].astype(jnp.bfloat16).reshape(length_value, head_number, -1)
    key_rows = sum_values[1].astype(jnp.bfloat16).reshape(length_value, head_number, -1)
    value_rows = sum_values[2].astype(jnp.bfloat16).reshape(length_value, head_number, value_dim)
    low_rank = jnp.dot(
        normalized_input, forget_left_factor, preferred_element_type=jnp.float32
    ).astype(jnp.bfloat16)
    gate_preactivation = (
        jnp.dot(low_rank, forget_right_factor, preferred_element_type=jnp.float32)
        + forget_offset_per_feature
    )
    forget_log_rate = (jax.nn.log_sigmoid(gate_preactivation) / softness_scale).reshape(
        length_value, head_number, -1
    )
    forget_log_rate = forget_log_rate + jnp.transpose(forget_spike_additions)[:, :, None]
    local_out, query_decayed, block_end, final_state = block_terms(
        query_rows, key_rows, value_rows, forget_log_rate
    )
    prefix = jnp.cumsum(block_end, axis=0) - block_end
    query_far = query_decayed * jnp.exp(prefix)[:, None]
    total_decay = jnp.exp(jnp.sum(block_end, axis=0))
    identity = (jnp.ones_like(total_decay), jnp.zeros_like(final_state))
    incoming = entering((total_decay, final_state), SP, chain_combine, identity)[1]
    attended = local_out + jnp.einsum(
        "nihd,hdv->nihv", query_far, incoming, precision=lax.Precision.HIGHEST
    )
    attended = attended.reshape(length_value, head_number, value_dim)
    return (
        norm_values(attended, subspace_rescale_vector)
        .astype(jnp.bfloat16)
        .reshape(length_value, head_number * value_dim)
    )


def conv_branch(sum_values, depthwise_filter_taps):
    outer = sum_values[0].astype(jnp.bfloat16)
    inner = sum_values[1].astype(jnp.bfloat16)
    conv_in = sum_values[2].astype(jnp.bfloat16)
    length_value = outer.shape[0]
    gated_in = (inner.astype(jnp.float32) * conv_in.astype(jnp.float32)).astype(jnp.bfloat16)
    reach = depthwise_filter_taps.shape[0] - 1
    rim_rows = shifted(gated_in[length_value - reach :], SP, 1)
    padded = jnp.concatenate([rim_rows, gated_in], axis=0)
    taps_f32 = depthwise_filter_taps.astype(jnp.float32)
    conv_sum = jnp.zeros(outer.shape, jnp.float32)
    for tap_index in range(depthwise_filter_taps.shape[0]):
        conv_sum = conv_sum + taps_f32[tap_index] * padded[
            tap_index : tap_index + length_value
        ].astype(jnp.float32)
    return (conv_sum * outer.astype(jnp.float32)).astype(jnp.bfloat16)


def body(
    hidden_activations,
    entry_rescale_vector,
    probe_matrix,
    lookup_address_matrix,
    payload_matrix,
    postfilter_switch_matrix,
    prefilter_switch_matrix,
    filter_source_matrix,
    forget_left_factor,
    forget_right_factor,
    forget_offset_per_feature,
    forget_spike_additions,
    subspace_rescale_vector,
    depthwise_filter_taps,
    mixer_result_matrix,
    filter_result_matrix,
):
    normalized_input = row_norm(
        entry_rescale_vector, lax.all_gather(hidden_activations, "tp", axis=0, tiled=True)
    )
    accumulate = project_rows(normalized_input)
    attn_sums = accumulate(
        empty_slots(normalized_input, (probe_matrix, lookup_address_matrix, payload_matrix)),
        in_one_piece((probe_matrix, lookup_address_matrix, payload_matrix), SP, 0, 1),
        jnp.int32(0),
    )
    mixed_attn = attention_path(
        normalized_input,
        attn_sums,
        forget_left_factor,
        forget_right_factor,
        forget_offset_per_feature,
        forget_spike_additions,
        subspace_rescale_vector,
    )
    conv_sums = accumulate(
        empty_slots(
            normalized_input,
            (postfilter_switch_matrix, prefilter_switch_matrix, filter_source_matrix),
        ),
        in_one_piece(
            (postfilter_switch_matrix, prefilter_switch_matrix, filter_source_matrix), SP, 0, 1
        ),
        jnp.int32(0),
    )
    mixed_conv = conv_branch(conv_sums, depthwise_filter_taps)
    return lax.psum_scatter(
        (
            jnp.dot(mixed_attn, mixer_result_matrix, preferred_element_type=jnp.float32)
            + jnp.dot(mixed_conv, filter_result_matrix, preferred_element_type=jnp.float32)
        ).astype(jnp.bfloat16),
        "tp",
        scatter_dimension=0,
        tiled=True,
    )


def solution(mesh):
    split = Mesh(mesh.devices.reshape(4, 4, mesh.shape["tp"]), ("sp_0", "sp_1", "tp"))
    in_specs = (
        P(SP_TP, None),
        P(),
        P(SP, "tp"),
        P(SP, "tp"),
        P(SP, "tp"),
        P(SP, "tp"),
        P(SP, "tp"),
        P(SP, "tp"),
        P(),
        P(None, "tp"),
        P("tp"),
        P("tp", SP),
        P("tp", None),
        P(None, "tp"),
        P("tp", None),
        P("tp", None),
    )
    out_specs = P(SP_TP, None)
    return jax.shard_map(body, mesh=split, in_specs=in_specs, out_specs=out_specs, check_vma=False)
```

profile of v0, /device:TPU:1, one launch (start us, length us, event | category | flops | bytes accessed | tf_op | source)
XLA Modules:
  0.0 311.4 jit_solution(12454789588959216576)
XLA Ops:
  6.6 0.7 all-gather.7.cloned.1.call-update
  7.3 1.9 pad_maximum_fusion.3
  9.3 2.1 pad_maximum_fusion.2
  11.8 41.7 %all-gather.7.cloned.1.call-done = bf16[768,4096]{1,0:T(8,128)(2,1)} async-done(((bf16[96,4096]{1,0:T(8,128)(2,1)}), bf16[768,4096]{1,0:T(8,128)(2,1)}) %all-gather.7.cloned.1.call-update) | async-done | bytes 6291472 | tf_op jit(solution)/shard_map/all_gather | solution.py:206
  53.5 4.2 %fusion = f32[768]{0:T(1024)S(1)} fusion(bf16[768,4096]{1,0:T(8,128)(2,1)} %all-gather.7.cloned.1.call-done), kind=kLoop, calls=%fused_computation.6 | loop fusion | flops 9436416 | bytes 6294528 | tf_op jit(solution)/shard_map/reduce_sum | solution.py:60
  57.7 0.4 copy-done.2
  58.1 5.4 %fusion.2 = bf16[768,4096]{1,0:T(8,128)(2,1)} fusion(bf16[768,4096]{1,0:T(8,128)(2,1)S(1)} %copy-done.2, f32[4096]{0:T(1024)S(1)} %convert_element_type.265, f32[768]{0:T(1024)S(1)} %add_rsqrt_fusion.1), kind=kLoop, calls=%fused_computation.8 | loop fusion | flops 12582912 | bytes 12602368 | tf_op jit(solution)/shard_map/convert_element_type | solution.py:65
  63.5 5.7 %fusion.49 = f32[768,256]{1,0:T(8,128)S(1)} fusion(bf16[64,256]{1,0:T(8,128)(2,1)S(1)} %copy-done.13, bf16[768,4096]{1,0:T(8,128)(2,1)} %fusion.2, bf16[4096,64]{0,1:T(8,128)(2,1)S(1)} %copy-done, f32[256]{0:T(256)S(1)} %copy-done.14), kind=kOutput, calls=%fused_computation.51 | convolution fusion | flops 429834240 | bytes 7635968 | tf_op jit(solution)/shard_map/dot_general | solution.py:143
  69.3 0.4 reshape.175
  69.7 0.7 fusion.45
  70.5 8.2 %all-gather.2 = bf16[4,2,128]{2,1,0:T(2,128)(2,1)S(1)} all-gather(bf16[1,2,128]{2,1,0:T(2,128)(2,1)S(1)} %fusion.121), channel_id=2, replica_groups=mesh['sp_0'=4,'sp_1'=4,'tp'=8] {'sp_1'}, dimensions={0}, use_global_device_ids=true | all-gather | bytes 2560 | tf_op jit(solution)/shard_map/all_gather | solution.py:28
  78.7 8.3 %all_gather.30 = bf16[4,2,128]{2,1,0:T(2,128)(2,1)S(1)} all-gather(bf16[1,2,128]{2,1,0:T(2,128)(2,1)S(1)} %get-tuple-element.96), channel_id=1, replica_groups=mesh['sp_0'=4,'sp_1'=4,'tp'=8] {'sp_0'}, dimensions={0}, use_global_device_ids=true | all-gather | bytes 2560 | tf_op jit(solution)/shard_map/all_gather | solution.py:28
  87.0 39.1 %all-gather.9.cloned.1.call-done = bf16[4096,1024]{1,0:T(8,128)(2,1)} async-done(((bf16[256,1024]{1,0:T(8,128)(2,1)}), bf16[4096,1024]{1,0:T(8,128)(2,1)}) %all-gather.9.cloned.1.call-update) | async-done | bytes 8388624 | tf_op jit(solution)/shard_map/all_gather | solution.py:51
  126.1 5.2 %fusion.42 = f32[768,256]{1,0:T(8,128)S(1)} fusion(bf16[768,4096]{1,0:T(8,128)(2,1)} %fusion.2, bf16[4096,1024]{1,0:T(8,128)(2,1)} %all-gather.9.cloned.1.call-done), kind=kOutput, calls=%fused_computation.39 | convolution fusion | flops 1611005952 | bytes 9175040 | tf_op jit(solution)/shard_map/dot_general | solution.py:73
  131.3 0.4 reshape.177
  131.7 7.4 %fusion.15 = bf16[768,512]{1,0:T(8,128)(2,1)S(1)} fusion(bf16[768,4096]{1,0:T(8,128)(2,1)} %fusion.2, bf16[4096,1024]{1,0:T(8,128)(2,1)} %all-gather.9.cloned.1.call-done), kind=kOutput, calls=%fused_computation.28 | convolution fusion | flops 3221618688 | bytes 11272192 | tf_op jit(solution)/shard_map/dot_general | solution.py:73
  139.2 0.2 reshape.174
  139.4 5.4 %fusion.36 = f32[768,256]{1,0:T(8,128)S(1)} fusion(bf16[768,4096]{1,0:T(8,128)(2,1)} %fusion.2, bf16[4096,1024]{1,0:T(8,128)(2,1)} %all-gather.9.cloned.1.call-done), kind=kOutput, calls=%fused_computation.37 | convolution fusion | flops 1611202560 | bytes 9175040 | tf_op jit(solution)/shard_map/dot_general | solution.py:73
  144.7 1.3 mul.250
  146.0 3.9 %copy_multiply_fusion = (f32[12,64,2,128]{3,0,1,2:T(8,128)S(1)}, f32[12,64,2,128]{3,0,1,2:T(8,128)}, f32[12,64,2,128]{3,0,1,2:T(8,128)}, f32[12,64,2,128]{3,0,1,2:T(8,128)S(1)}) fusion(f32[12,64,2,128]{3,2,1,0:T(2,128)S(1)} %reshape.177, f32[12,64,2,128]{3,0,1,2:T(8,128)} %copy-done.5, f32[12,2,128]{2,0,1:T(8,128)S(1)} %get-tuple-element.140, ...), kind=kLoop, calls=%fused_computation.41 | loop fusion | flops 1179648 | bytes 5529600 | tf_op jit(solution)/shard_map/mul | solution.py:102
  149.9 3.2 %fusion.52 = f32[12,2,128,256]{3,2,1,0:T(8,128)} fusion(f32[12,64,2,128]{3,0,1,2:T(8,128)S(1)} %get-tuple-element.85, bf16[12,64,2,256]{3,2,1,0:T(2,128)(2,1)S(1)} %reshape.174), kind=kOutput, calls=%fused_computation.56 | convolution fusion | flops 603979776 | bytes 4718592 | tf_op jit(solution)/shard_map/njhd,njhv->nhdv/dot_general | solution.py:108
  153.1 22.3 %while.13 = (s32[]{:T(128)}, f32[2,128,256]{2,1,0:T(8,128)S(1)}, f32[12,2,128,256]{3,2,1,0:T(8,128)}, f32[12,2,128]{2,0,1:T(8,128)S(1)}, f32[12,2,128,256]{3,2,1,0:T(8,128)}, /*index=5*/s32[]{:T(128)}, s32[]{:T(128)}) while((s32[]{:T(128)}, f32[2,128,256]{2,1,0:T(8,128)S(1)}, f32[12,2,128,256]{3,2,1,0:T(8,128)}, ...), condition=%wide.region_3.4_spmd.clone, body=%wide.region_2.3_spmd.clone.sunk | while | flops 262147 | bytes 1315948 | solution.py:115
  153.1 0.7 bitcast_dynamic-update-slice_fusion.2
  153.8 1.1 bitcast_add_fusion.3
  154.9 0.7 bitcast_dynamic-update-slice_fusion.2
  155.7 1.1 bitcast_add_fusion.3
  156.8 0.7 bitcast_dynamic-update-slice_fusion.2
  157.5 1.1 bitcast_add_fusion.3
  158.6 0.7 bitcast_dynamic-update-slice_fusion.2
  159.4 1.1 bitcast_add_fusion.3
  160.5 0.7 bitcast_dynamic-update-slice_fusion.2
  161.2 1.1 bitcast_add_fusion.3
  162.3 0.7 bitcast_dynamic-update-slice_fusion.2
  163.1 1.1 bitcast_add_fusion.3
  164.2 0.7 bitcast_dynamic-update-slice_fusion.2
  164.9 1.1 bitcast_add_fusion.3
  166.1 0.7 bitcast_dynamic-update-slice_fusion.2
  166.8 1.1 bitcast_add_fusion.3
  168.0 0.7 bitcast_dynamic-update-slice_fusion.2
  168.7 1.1 bitcast_add_fusion.3
  169.8 0.7 bitcast_dynamic-update-slice_fusion.2
  170.5 1.1 bitcast_add_fusion.3
  171.6 0.7 bitcast_dynamic-update-slice_fusion.2
  172.4 1.1 bitcast_add_fusion.3
  173.5 0.7 bitcast_dynamic-update-slice_fusion.2
  174.2 1.1 bitcast_add_fusion.3
  175.4 14.8 %all-gather.1 = bf16[8,128,256]{2,1,0:T(8,128)(2,1)S(1)} all-gather(bf16[2,128,256]{2,1,0:T(8,128)(2,1)S(1)} %convert_element_type.296), channel_id=3, replica_groups=mesh['sp_0'=4,'sp_1'=4,'tp'=8] {'sp_1'}, dimensions={0}, use_global_device_ids=true | all-gather | bytes 655360 | tf_op jit(solution)/shard_map/all_gather | solution.py:28
  190.2 0.2 fusion.81
  190.4 14.6 %all_gather.33 = bf16[4,2,128,256]{3,2,1,0:T(8,128)(2,1)S(1)} all-gather(bf16[1,2,128,256]{3,2,1,0:T(8,128)(2,1)S(1)} %fusion.81), channel_id=1, replica_groups=mesh['sp_0'=4,'sp_1'=4,'tp'=8] {'sp_0'}, dimensions={0}, use_global_device_ids=true | all-gather | bytes 655360 | tf_op jit(solution)/shard_map/all_gather | solution.py:28
  205.0 3.1 convolution_select_fusion
  208.1 0.8 fusion.60
  208.9 2.1 fusion.62
  211.0 3.4 %multiply_reduce_fusion = (f32[12,64,2]{1,2,0:T(2,128)S(1)}, f32[12,64,2,256]{3,1,2,0:T(8,128)}) fusion(f32[12,64,2,128]{3,0,1,2:T(8,128)S(1)} %copy-done.7, bf16[4,2,128,256]{3,2,1,0:T(8,128)(2,1)S(1)} %all_gather.33, f32[2,128]{1,0:T(2,128)S(1)} %get-tuple-element.97, f32[2,128]{1,0:T(2,128)S(1)} %get-tuple-element.103, ...), kind=kOutput, calls=%fused_computation.27 | convolution fusion | flops 607648256 | bytes 6568968 | tf_op jit(solution)/shard_map/nihd,hdv->nihv/dot_general | solution.py:158
  214.4 0.2 copy.72
  214.6 1.2 mul.290
  216.0 1.2 copy.69
  217.2 1.3 copy.75
  218.5 3.5 %all-gather.11.cloned.1.call-done = bf16[4096,1536]{1,0:T(8,128)(2,1)} async-done(((bf16[256,1536]{1,0:T(8,128)(2,1)}), bf16[4096,1536]{1,0:T(8,128)(2,1)}) %all-gather.11.cloned.1.call-update) | async-done | bytes 12582928 | tf_op jit(solution)/shard_map/all_gather | solution.py:51
  222.0 7.4 %fusion.18 = bf16[768,512]{1,0:T(8,128)(2,1)S(1)} fusion(bf16[768,4096]{1,0:T(8,128)(2,1)} %fusion.2, bf16[4096,1536]{1,0:T(8,128)(2,1)} %all-gather.11.cloned.1.call-done), kind=kOutput, calls=%fused_computation.29 | convolution fusion | flops 3221618688 | bytes 11272192 | tf_op jit(solution)/shard_map/dot_general | solution.py:73
  229.4 7.6 %multiply_convert_fusion.1 = bf16[768,512]{1,0:T(8,128)(2,1)S(1)} fusion(bf16[768,512]{1,0:T(8,128)(2,1)S(1)} %fusion.18, bf16[768,4096]{1,0:T(8,128)(2,1)} %fusion.2, bf16[4096,1536]{1,0:T(8,128)(2,1)} %all-gather.11.cloned.1.call-done), kind=kOutput, calls=%fused_computation.25 | convolution fusion | flops 3223191552 | bytes 12058624 | tf_op jit(solution)/shard_map/dot_general | solution.py:73
  237.0 3.1 collective-permute-start
  240.2 6.4 %fusion.47 = f32[768,4096]{1,0:T(8,128)} fusion(bf16[512,4096]{1,0:T(8,128)(2,1)S(1)} %copy-done.6, f32[768,512]{1,0:T(8,128)S(1)} %bitcast.180, f32[768,512]{1,0:T(8,128)S(1)} %bitcast.179, f32[512]{0:T(512)S(1)} %bitcast.185), kind=kOutput, calls=%fused_computation.49 | convolution fusion | flops 3222405120 | bytes 19924992 | tf_op jit(solution)/shard_map/dot_general | solution.py:236
  246.6 15.3 %add_convert_fusion = bf16[768,4096]{1,0:T(8,128)(2,1)} fusion(f32[768,4096]{1,0:T(8,128)} %fusion.47, bf16[512,4096]{1,0:T(8,128)(2,1)} %param.33, bf16[768,512]{1,0:T(8,128)(2,1)S(1)} %multiply_convert_fusion.1, bf16[2,512]{1,0:T(2,128)(2,1)S(1)} %collective-permute-done, f32[512]{0:T(512)S(1)} %bitcast.189, f32[512]{0:T(512)S(1)} %bitcast.188, ...), kind=kOutput, calls=%fused_computation.9 | convolution fusion | flops 6455820288 | bytes 34349056 | tf_op jit(solution)/shard_map/dot_general | solution.py:237
  261.9 43.0 %reduce-scatter.2.cloned.1.call-done = bf16[96,4096]{1,0:T(8,128)(2,1)} async-done(((bf16[768,4096]{1,0:T(8,128)(2,1)}), bf16[96,4096]{1,0:T(8,128)(2,1)}) %reduce-scatter.2.cloned.1.call-update) | async-done | bytes 786448 | tf_op jit(solution)/shard_map/reduce_scatter | solution.py:234
  (83 shorter events, 0.9 us)
Async XLA Ops:
  6.5 57.0 %copy-start = (bf16[4096,64]{0,1:T(8,128)(2,1)S(1)}, bf16[4096,64]{0,1:T(8,128)(2,1)}, u32[]{:S(2)}) copy-start(bf16[4096,64]{0,1:T(8,128)(2,1)} %param.26) | copy-start | bytes 1572868
  6.5 4.9 %copy-start.12 = (bf16[2,256]{1,0:T(2,128)(2,1)S(1)}, bf16[2,256]{1,0:T(2,128)(2,1)}, u32[]{:S(2)}) copy-start(bf16[2,256]{1,0:T(2,128)(2,1)} %param.30) | copy-start | bytes 3076
  6.5 5.0 %copy-start.10 = (bf16[4096]{0:T(1024)(128)(2,1)S(1)}, bf16[4096]{0:T(1024)(128)(2,1)}, u32[]{:S(2)}) copy-start(bf16[4096]{0:T(1024)(128)(2,1)} %param.19) | copy-start | bytes 24580
  6.5 5.0 %copy-start.11 = (f32[2,768]{1,0:T(2,128)S(1)}, f32[2,768]{1,0:T(2,128)}, u32[]{:S(2)}) copy-start(f32[2,768]{1,0:T(2,128)} %param.29) | copy-start | bytes 18436
  6.5 5.2 %copy-start.9 = (bf16[3,512]{1,0:T(4,128)(2,1)S(1)}, bf16[3,512]{1,0:T(4,128)(2,1)}, u32[]{:S(2)}) copy-start(bf16[3,512]{1,0:T(4,128)(2,1)} %param.31) | copy-start | bytes 9220
  6.5 46.9 %all-gather.7.cloned.1.call-start = ((), (), s32[]{:S(2)}) async-start(), calls=%async_computation.1 | async-start | bytes 7077888 | tf_op jit(solution)/shard_map/all_gather | solution.py:206
  7.3 118.8 %all-gather.9.cloned.1.call-start = ((), (), s32[]{:S(2)}) async-start(), calls=%async_computation.2 | async-start | bytes 8912896 | tf_op jit(solution)/shard_map/all_gather | solution.py:51
  9.2 212.8 %all-gather.11.cloned.1.call-start = ((), (), s32[]{:S(2)}) async-start(), calls=%async_computation.3 | async-start | bytes 13369344 | tf_op jit(solution)/shard_map/all_gather | solution.py:51
  11.4 293.5 %reduce-scatter.2.cloned.1.call-start = ((), (), s32[]{:S(2)}) async-start(), calls=%async_computation.4 | async-start | bytes 7077888 | tf_op jit(solution)/shard_map/reduce_scatter | solution.py:234
  53.5 4.6 %copy-start.2 = (bf16[768,4096]{1,0:T(8,128)(2,1)S(1)}, bf16[768,4096]{1,0:T(8,128)(2,1)}, u32[]{:S(2)}) copy-start(bf16[768,4096]{1,0:T(8,128)(2,1)} %all-gather.7.cloned.1.call-done) | copy-start | bytes 18874372
  58.1 5.4 %copy-start.13 = (bf16[64,256]{1,0:T(8,128)(2,1)S(1)}, bf16[64,256]{1,0:T(8,128)(2,1)}, u32[]{:S(2)}) copy-start(bf16[64,256]{1,0:T(8,128)(2,1)} %param.27) | copy-start | bytes 98308
  58.1 5.4 %copy-start.14 = (f32[256]{0:T(256)S(1)}, f32[256]{0:T(256)}, u32[]{:S(2)}) copy-start(f32[256]{0:T(256)} %param.28) | copy-start | bytes 3076
  70.4 60.9 %copy-start.5 = (f32[12,64,2,128]{3,0,1,2:T(8,128)}, f32[12,64,2,128]{3,0,1,2:T(8,128)S(1)}, u32[]{:S(2)}) copy-start(f32[12,64,2,128]{3,0,1,2:T(8,128)S(1)} %fusion.45) | copy-start | bytes 2359300
  175.3 33.6 %copy-start.8 = (f32[12,2,128,256]{3,2,1,0:T(8,128)S(1)}, f32[12,2,128,256]{3,2,1,0:T(8,128)}, u32[]{:S(2)}) copy-start(f32[12,2,128,256]{3,2,1,0:T(8,128)} %get-tuple-element.33) | copy-start | bytes 9437188
  208.1 2.9 copy-start.7
  214.6 1.4 copy-start.4
  229.4 10.7 %copy-start.3 = (f32[96,8,2,256]{3,1,2,0:T(8,128)S(1)}, f32[96,8,2,256]{3,1,2,0:T(8,128)}, u32[]{:S(2)}) copy-start(f32[96,8,2,256]{3,1,2,0:T(8,128)} %copy.75) | copy-start | bytes 4718596
  229.4 10.7 %copy-start.6 = (bf16[512,4096]{1,0:T(8,128)(2,1)S(1)}, bf16[512,4096]{1,0:T(8,128)(2,1)}, u32[]{:S(2)}) copy-start(bf16[512,4096]{1,0:T(8,128)(2,1)} %param.32) | copy-start | bytes 12582916
  237.0 9.5 %collective-permute-start = (bf16[2,512]{1,0:T(2,128)(2,1)S(1)}, bf16[2,512]{1,0:T(2,128)(2,1)S(1)}, u32[]{:S(2)}, u32[]{:S(2)}) collective-permute-start(bf16[2,512]{1,0:T(2,128)(2,1)S(1)} %slice.151), channel_id=1, source_target_pairs={{0,8},{8,16},{16,24},{24,32},{32,40},{40,48},{48,56},{56,64},{64,7... | collective-permute-start | bytes 6152 | tf_op jit(solution)/shard_map/ppermute | solution.py:46
  246.6 58.4 %copy-start.1 = (bf16[4096,64]{0,1:T(8,128)(2,1)S(1)}, bf16[4096,64]{0,1:T(8,128)(2,1)}, u32[]{:S(2)}) copy-start(bf16[4096,64]{0,1:T(8,128)(2,1)} %param.26) | copy-start | bytes 1572868
Sparse Core Ops, SparseCore 0:
  9.0 44.4 all-gather.6
  55.6 70.4 all-gather.8
  128.3 93.7 all-gather.10
  262.0 42.8 reduce-scatter.1
where the time goes:
time: 312 us; the launch traced here: 311 us
  waiting for transfers between devices  128 us (41%)
  matrix products  72.9 us (23%)
  blocking collectives  45.9 us (15%)
  other arithmetic  40.2 us (13%)
  between operations  13.5 us (4%)
  local copies, waits for them, and re-layouts  7.15 us (2%)
  starting transfers between devices  3.27 us (1%)
    all_gather x4, blocking collectives, entering(): lax.all_gather(part.astype(kind), axis)  45.9 us
    reduce_scatter x1, waiting for transfers between devices, body(): lax.psum_scatter((jnp.dot(mixed_attn, mixer_result_matrix, preferred_elem...  43 us
    all_gather x2, waiting for transfers between devices, in_one_piece(): lax.all_gather(both, axis, axis=dim, tiled=True)  42.6 us
    all_gather x1, waiting for transfers between devices, body(): lax.all_gather(hidden_activations, 'tp', axis=0, tiled=True)  41.7 us
    dot_general x5, matrix products, accumulate(): jnp.dot(normalized_input, rows_now, preferred_element_type=jnp.float32)  32.9 us
    dot_general x1, matrix products, body(): jnp.dot(mixed_conv, filter_result_matrix, preferred_element_type=jnp.floa...  15.3 us
    add x12, other arithmetic, advance(): return (jnp.exp(decay_now)[..., None] * state + update_now, state)  12.9 us
    dynamic_update_slice x12, other arithmetic, block_terms(): final_state, state_in = lax.scan(advance, start_state, (block_end, updates))  8.77 us
  transfers between devices with their start and end apart: 5, of which 4 were waited for; matrix products, arithmetic and copies ran while one was open for 29% of the time, Pallas kernels for 0%

commit v1 on v0

v1 whole, which is shorter than its diff:
```python
import functools

import jax
import jax.numpy as jnp
from jax import lax
from jax.experimental import pallas as pl
from jax.experimental.pallas import tpu as pltpu
from jax.sharding import Mesh
from jax.sharding import PartitionSpec as P

MESH = pl.DeviceIdType.MESH
SP = ("sp_0", "sp_1")
SP_TP = ("sp_0", "sp_1", "tp")
F32 = jnp.float32
BF16 = jnp.bfloat16
HIGHEST = lax.Precision.HIGHEST

BLOCK = 64
ROWS = 96
TOK = 768
MODEL = 4096
KB = 256
QA, CA = 512, 768
KEY, VAL = 128, 256
EPS = 1e-06
DELTA = (0, 3, 1, 2)


def nt(a, b):
    return lax.dot_general(a, b, (((1,), (1,)), ((), ())), preferred_element_type=F32)


def tn(a, b):
    return lax.dot_general(a, b, (((0,), (0,)), ((), ())), preferred_element_type=F32)


def mm(a, b):
    return jnp.dot(a, b, preferred_element_type=F32)


def front_kernel(
    x_in,
    gain,
    w_q,
    w_k,
    w_v,
    w_out,
    w_in,
    w_src,
    left,
    right,
    offset,
    spikes,
    head_gain,
    taps,
    attn_out,
    conv_out,
    xs,
    qa,
    qb,
    ca,
    cb,
    acc_a,
    acc_b,
    qrows,
    krows,
    vrows,
    rate,
    inside,
    q_far,
    state,
    prefix,
    st_send,
    dec_send,
    st_recv,
    dec_recv,
    gated,
    load_sem,
    w_send,
    w_recv,
    x_send,
    x_recv,
    s_send,
    s_recv,
    h_sem,
):
    z = lax.axis_index("sp_0")
    y = lax.axis_index("sp_1")
    t = lax.axis_index("tp")
    core = t % 2
    xi = t // 2
    sib = xi * 2 + (1 - core)

    def at_z(d):
        return {"sp_0": (z + d) % 4}

    def at_y(d):
        return {"sp_1": (y + d) % 4}

    def at_x(d):
        return {"tp": ((xi + d) % 4) * 2 + core}

    sp = z * 4 + y
    sp_next = (sp + 1) % 16
    sp_prev = (sp + 15) % 16
    to_next = {"sp_0": sp_next // 4, "sp_1": sp_next % 4}
    to_prev = {"sp_0": sp_prev // 4, "sp_1": sp_prev % 4}
    to_sib = {"tp": sib}

    own = pl.ds(pl.multiple_of(sp * KB, KB), KB)
    own_rows = pl.multiple_of(t * ROWS, 32)
    loads = [
        pltpu.make_async_copy(x_in, xs.at[pl.ds(own_rows, ROWS), :], load_sem.at[0]),
        pltpu.make_async_copy(w_q, qa.at[own, 0:256], load_sem.at[1]),
        pltpu.make_async_copy(w_k, qa.at[own, 256:512], load_sem.at[2]),
        pltpu.make_async_copy(w_v, qb.at[own, :], load_sem.at[3]),
        pltpu.make_async_copy(w_out, ca.at[own, 0:512], load_sem.at[4]),
        pltpu.make_async_copy(w_in.at[:, 0:256], ca.at[own, 512:768], load_sem.at[5]),
        pltpu.make_async_copy(w_in.at[:, 256:512], cb.at[own, 0:256], load_sem.at[6]),
        pltpu.make_async_copy(w_src, cb.at[own, 256:768], load_sem.at[7]),
    ]
    for c in loads:
        c.start()

    barrier = pltpu.get_barrier_semaphore()
    peers = [at_z(1), at_z(2), at_z(3), at_y(1), at_y(2), at_y(3), at_x(1), at_x(3), to_sib, to_next, to_prev]
    for p in peers:
        pl.semaphore_signal(barrier, inc=1, device_id=p, device_id_type=MESH)

    loads[0].wait()

    def norm_rows(i, _):
        r = pl.ds(pl.multiple_of(own_rows + i * 16, 16), 16)
        v = xs[r, :].astype(F32)
        ms = jnp.mean(v * v, axis=-1, keepdims=True)
        xs[r, :] = (v * lax.rsqrt(ms + EPS) * gain[...]).astype(BF16)
        return 0

    lax.fori_loop(0, ROWS // 16, norm_rows, 0)
    for c in loads[1:]:
        c.wait()
    pl.semaphore_wait(barrier, len(peers))

    def x_copy(slot, sender_x, row, rows, dst, sender_core=None):
        g = sender_x * 2 + (core if sender_core is None else sender_core)
        ref = xs.at[pl.ds(pl.multiple_of(g * ROWS + row, 16), rows), :]
        return pltpu.make_async_remote_copy(
            src_ref=ref,
            dst_ref=ref,
            send_sem=x_send.at[slot],
            recv_sem=x_recv.at[slot],
            device_id=dst,
            device_id_type=MESH,
        )

    started = []

    def go(c):
        c.start()
        started.append(c)

    right_x, left_x = at_x(1), at_x(3)
    xm, xp, xf = (xi + 3) % 4, (xi + 1) % 4, (xi + 2) % 4

    bufs = {("q", 0): qa, ("q", 1): qb, ("c", 0): ca, ("c", 1): cb}

    def blk(path, du, dv, row=0, rows=KB):
        if path == 0:
            j = ((z + du) % 4) * 4 + (y + dv) % 4
        else:
            j = ((z + dv) % 4) * 4 + (y + du) % 4
        return pl.ds(pl.multiple_of(j * KB + row, 128), rows)

    def w_copy(group, path, slot, du, dv, axis, step, row=0, rows=KB):
        ref = bufs[group, path].at[blk(path, du, dv, row, rows), :]
        along_z = (axis == 0) == (path == 0)
        s = (0 if group == "q" else 2) + path
        return pltpu.make_async_remote_copy(
            src_ref=ref,
            dst_ref=ref,
            send_sem=w_send.at[s, slot],
            recv_sem=w_recv.at[s, slot],
            device_id=at_z(step) if along_z else at_y(step),
            device_id_type=MESH,
        )

    def send_first(g):
        for p in (0, 1):
            go(w_copy(g, p, 0, 0, 0, 0, 1))
            go(w_copy(g, p, 1, 0, 0, 0, 3))

    def wait_first(g):
        for p in (0, 1):
            w_copy(g, p, 0, 3, 0, 0, 1).wait_recv()
            go(w_copy(g, p, 2, 3, 0, 0, 1, 0, 128))
            w_copy(g, p, 1, 1, 0, 0, 3).wait_recv()
            go(w_copy(g, p, 3, 1, 0, 0, 3, 128, 128))

    def wait_first_halves(g):
        for p in (0, 1):
            w_copy(g, p, 2, 2, 0, 0, 1, 0, 128).wait_recv()
            w_copy(g, p, 3, 2, 0, 0, 3, 128, 128).wait_recv()

    def send_second(g, k):
        for p in (0, 1):
            go(w_copy(g, p, 4 + 2 * k, DELTA[k], 0, 1, 1))
            go(w_copy(g, p, 5 + 2 * k, DELTA[k], 0, 1, 3))

    def wait_second(g, k):
        for p in (0, 1):
            w_copy(g, p, 4 + 2 * k, DELTA[k], 3, 1, 1).wait_recv()
            go(w_copy(g, p, 12 + 2 * k, DELTA[k], 3, 1, 1, 0, 128))
            w_copy(g, p, 5 + 2 * k, DELTA[k], 1, 1, 3).wait_recv()
            go(w_copy(g, p, 13 + 2 * k, DELTA[k], 1, 1, 3, 128, 128))

    def wait_second_halves(g, k):
        for p in (0, 1):
            w_copy(g, p, 12 + 2 * k, DELTA[k], 2, 1, 1, 0, 128).wait_recv()
            w_copy(g, p, 13 + 2 * k, DELTA[k], 2, 1, 3, 128, 128).wait_recv()

    def project(g, k, acc_list, width):
        for p in (0, 1):
            acc = acc_list[p]
            w = bufs[g, p]

            def tile(i, _, acc=acc, w=w, p=p):
                r = pl.ds(pl.multiple_of((i % 3) * 256, 256), 256)
                c = pl.ds(pl.multiple_of((i // 3) * 256, 256), 256)
                total = None
                for v in range(4):
                    if p == 0:
                        j = ((z + DELTA[k]) % 4) * 4 + v
                    else:
                        j = v * 4 + (y + DELTA[k]) % 4
                    at = pl.ds(pl.multiple_of(j * KB, KB), KB)
                    part = mm(xs[r, at], w[at, c])
                    total = part if total is None else total + part
                if k == 0:
                    acc[r, c] = total
                else:
                    acc[r, c] += total
                return 0

            lax.fori_loop(0, 3 * (width // 256), tile, 0)

    send_first("q")
    go(x_copy(0, xi, 0, 48, right_x))
    go(x_copy(2, xi, 48, 48, left_x))
    go(x_copy(1, xi, 48, 48, right_x))
    go(x_copy(3, xi, 0, 48, left_x))
    go(x_copy(6, xi, 0, ROWS, to_sib))
    send_second("q", 0)

    wait_first("q")
    send_second("q", 1)
    send_second("q", 2)
    x_copy(0, xm, 0, 48, right_x).wait_recv()
    go(x_copy(4, xm, 0, 48, right_x))
    x_copy(2, xp, 48, 48, left_x).wait_recv()
    go(x_copy(5, xp, 48, 48, left_x))
    wait_first_halves("q")
    send_second("q", 3)
    wait_second("q", 0)
    x_copy(1, xm, 48, 48, right_x).wait_recv()
    go(x_copy(7, xm, 0, ROWS, to_sib))
    x_copy(3, xp, 0, 48, left_x).wait_recv()
    go(x_copy(8, xp, 0, ROWS, to_sib))
    wait_second("q", 1)
    wait_second("q", 2)
    send_first("c")
    x_copy(4, xf, 0, 48, right_x).wait_recv()
    x_copy(5, xf, 48, 48, left_x).wait_recv()
    go(x_copy(9, xf, 0, ROWS, to_sib))
    wait_second("q", 3)
    send_second("c", 0)
    for slot, src in ((6, xi), (7, xm), (8, xp), (9, xf)):
        x_copy(slot, src, 0, ROWS, to_sib, 1 - core).wait_recv()

    def rates(i, _):
        r = pl.ds(pl.multiple_of(i * 128, 128), 128)
        low = mm(xs[r, :], left[...]).astype(BF16)
        g = mm(low, right[...]) + offset[...]
        ls = jnp.minimum(g, 0.0) - jnp.log1p(jnp.exp(-jnp.abs(g)))
        rate[r, :] = ls * (1.0 / 16.0) + spikes[r, :]
        return 0

    lax.fori_loop(0, TOK // 128, rates, 0)

    wait_first("c")
    send_second("c", 1)
    send_second("c", 2)
    for k in range(4):
        wait_second_halves("q", k)
        project("q", k, (acc_a, acc_b), QA)
    wait_first_halves("c")
    send_second("c", 3)

    def store_qkv(i, _):
        r = pl.ds(pl.multiple_of(i * 64, 64), 64)
        qrows[r, :] = acc_a[r, 0:256].astype(BF16)
        krows[r, :] = acc_a[r, 256:512].astype(BF16)
        vrows[r, :] = acc_b[r, 0:512].astype(BF16)
        return 0

    lax.fori_loop(0, TOK // 64, store_qkv, 0)

    state[...] = jnp.zeros_like(state)
    prefix[...] = jnp.zeros_like(prefix)

    def attend(n, _):
        r = pl.ds(pl.multiple_of(n * BLOCK, BLOCK), BLOCK)
        row = lax.broadcasted_iota(jnp.int32, (BLOCK, BLOCK), 0)
        col = lax.broadcasted_iota(jnp.int32, (BLOCK, BLOCK), 1)
        causal = row >= col
        within = lax.dot_general(
            jnp.where(causal, 1.0, 0.0).astype(F32),
            rate[r, :],
            (((1,), (0,)), ((), ())),
            precision=HIGHEST,
            preferred_element_type=F32,
        )
        end = within[BLOCK - 1 : BLOCK, :]
        mid = end * 0.5
        q_s = qrows[r, :].astype(F32) * (KEY**-0.5) * jnp.exp(within - mid)
        k_s = krows[r, :].astype(F32) * jnp.exp(mid - within)
        e_mid = jnp.exp(mid)
        q_d = q_s * e_mid
        k_t = (k_s * e_mid).astype(BF16)
        e_end = jnp.exp(end)
        before = prefix[0:1, :]
        q_far[r, :] = (q_d * jnp.exp(before)).astype(BF16)
        prefix[0:1, :] = before + end
        q_d = q_d.astype(BF16)
        q_s = q_s.astype(BF16)
        k_s = k_s.astype(BF16)
        for h in range(2):
            kc = slice(h * KEY, (h + 1) * KEY)
            vc = slice(h * VAL, (h + 1) * VAL)
            v = vrows[r, vc]
            scores = jnp.where(causal, nt(q_s[:, kc], k_s[:, kc]), 0.0).astype(BF16)
            s = state[vc, :]
            inside[r, vc] = mm(scores, v) + nt(q_d[:, kc], s.astype(BF16))
            state[vc, :] = s * e_end[:, kc] + tn(v, k_t[:, kc])
        return 0

    lax.fori_loop(0, 6, attend, 0)
    wait_second("c", 0)
    lax.fori_loop(6, 12, attend, 0)
    wait_second("c", 1)

    def st_copy(phase, d, dst):
        i = phase * 3 + d - 1
        return (
            pltpu.make_async_remote_copy(
                src_ref=st_send.at[phase],
                dst_ref=st_recv.at[i],
                send_sem=s_send.at[0, i],
                recv_sem=s_recv.at[0, i],
                device_id=dst,
                device_id_type=MESH,
            ),
            pltpu.make_async_remote_copy(
                src_ref=dec_send.at[phase],
                dst_ref=dec_recv.at[i],
                send_sem=s_send.at[1, i],
                recv_sem=s_recv.at[1, i],
                device_id=dst,
                device_id_type=MESH,
            ),
        )

    own_decay = jnp.exp(prefix[0:1, :])
    st_send[0] = state[...].astype(BF16)
    dec_send[0] = jnp.broadcast_to(own_decay, (8, 2 * KEY))
    wait_second("c", 2)
    for d in (1, 2, 3):
        for c in st_copy(0, d, at_y(d)):
            go(c)
    wait_second("c", 3)
    wait_second_halves("c", 0)
    project("c", 0, (acc_a, acc_b), CA)
    for d in (1, 2, 3):
        for c in st_copy(0, d, at_y(d)):
            c.wait_recv()

    def fold(total, decay, i, use):
        dec = jnp.where(use, dec_recv[i][0:1, :], 1.0)
        out = []
        for h in range(2):
            kc = slice(h * KEY, (h + 1) * KEY)
            vc = slice(h * VAL, (h + 1) * VAL)
            got = jnp.where(use, st_recv[i, vc, :].astype(F32), 0.0)
            out.append(total[h] * dec[:, kc] + got)
        return out, decay * dec

    before_y = [jnp.zeros((VAL, KEY), F32) for _ in range(2)]
    decay_y = jnp.ones((1, 2 * KEY), F32)
    for d in (3, 2, 1):
        before_y, decay_y = fold(before_y, decay_y, d - 1, d <= y)
    total = [
        before_y[h] * own_decay[:, h * KEY : (h + 1) * KEY] + state[h * VAL : (h + 1) * VAL, :]
        for h in range(2)
    ]
    decay_row = decay_y * own_decay
    for h in range(2):
        state[h * VAL : (h + 1) * VAL, :] = before_y[h]
    for d in (3, 2, 1):
        total, decay_row = fold(total, decay_row, d - 1, d > y)
    for h in range(2):
        st_send[1, h * VAL : (h + 1) * VAL, :] = total[h].astype(BF16)
    dec_send[1] = jnp.broadcast_to(decay_row, (8, 2 * KEY))
    prefix[1:2, :] = decay_y
    wait_second_halves("c", 1)
    for d in (1, 2, 3):
        for c in st_copy(1, d, at_z(d)):
            go(c)
    project("c", 1, (acc_a, acc_b), CA)
    wait_second_halves("c", 2)
    project("c", 2, (acc_a, acc_b), CA)
    for d in (1, 2, 3):
        for c in st_copy(1, d, at_z(d)):
            c.wait_recv()
    before_z = [jnp.zeros((VAL, KEY), F32) for _ in range(2)]
    decay_z = jnp.ones((1, 2 * KEY), F32)
    for d in (3, 2, 1):
        before_z, decay_z = fold(before_z, decay_z, 3 + d - 1, d <= z)
    decay_y = prefix[1:2, :]
    for h in range(2):
        vc = slice(h * VAL, (h + 1) * VAL)
        state[vc, :] = before_z[h] * decay_y[:, h * KEY : (h + 1) * KEY] + state[vc, :]

    def finish(n, _):
        r = pl.ds(pl.multiple_of(n * 128, 128), 128)
        for h in range(2):
            kc = slice(h * KEY, (h + 1) * KEY)
            vc = slice(h * VAL, (h + 1) * VAL)
            a = inside[r, vc] + nt(q_far[r, kc], state[vc, :].astype(BF16))
            ms = jnp.mean(a * a, axis=-1, keepdims=True)
            attn_out[r, vc] = (a * lax.rsqrt(ms + EPS) * head_gain[h : h + 1, :]).astype(BF16)
        return 0

    lax.fori_loop(0, TOK // 128, finish, 0)

    wait_second_halves("c", 3)
    project("c", 3, (acc_a, acc_b), CA)

    def gate(i, _):
        r = pl.ds(pl.multiple_of(i * 64, 64), 64)
        o = pl.ds(pl.multiple_of(i * 64 + 8, 8), 64)
        gated[o, 0:256] = (
            (acc_a[r, 512:768].astype(BF16).astype(F32) * acc_b[r, 256:512].astype(BF16).astype(F32))
            .astype(BF16)
            .astype(F32)
        )
        gated[o, 256:512] = (
            (acc_b[r, 0:256].astype(BF16).astype(F32) * acc_b[r, 512:768].astype(BF16).astype(F32))
            .astype(BF16)
            .astype(F32)
        )
        return 0

    lax.fori_loop(0, TOK // 64, gate, 0)
    halo = pltpu.make_async_remote_copy(
        src_ref=gated.at[pl.ds(TOK, 8), :],
        dst_ref=gated.at[pl.ds(0, 8), :],
        send_sem=h_sem.at[0],
        recv_sem=h_sem.at[1],
        device_id=to_next,
        device_id_type=MESH,
    )
    go(halo)

    def conv(first, i):
        r0 = i * 64
        block = gated[pl.ds(pl.multiple_of(r0, 8), 72), :]
        if first:
            keep = jnp.where(sp == 0, 0.0, 1.0)
            rim = lax.broadcasted_iota(jnp.int32, (72, 1), 0) < 8
            block = jnp.where(rim, block * keep, block)
        one = pltpu.roll(block, 1, 0)[8:, :]
        two = pltpu.roll(block, 2, 0)[8:, :]
        s = taps[0:1, :] * two + taps[1:2, :] * one + taps[2:3, :] * block[8:, :]
        r = pl.ds(pl.multiple_of(r0, 64), 64)
        outer = acc_a[r, 0:512].astype(BF16).astype(F32)
        conv_out[r, :] = (s * outer).astype(BF16)

    def conv_step(i, _):
        conv(False, i)
        return 0

    lax.fori_loop(1, TOK // 64, conv_step, 0)
    halo.wait_recv()
    conv(True, 0)
    for c in started:
        c.wait_send()


def front(*args):
    any_ = pl.BlockSpec(memory_space=pl.ANY)
    vmem = pl.BlockSpec(memory_space=pltpu.VMEM)
    dma = pltpu.SemaphoreType.DMA
    return pl.pallas_call(
        front_kernel,
        out_shape=(
            jax.ShapeDtypeStruct((TOK, 2 * VAL), BF16),
            jax.ShapeDtypeStruct((TOK, 512), BF16),
        ),
        in_specs=[any_, vmem] + [any_] * 6 + [vmem] * 6,
        out_specs=(vmem, vmem),
        scratch_shapes=[
            pltpu.VMEM((TOK, MODEL), BF16),
            pltpu.VMEM((MODEL, QA), BF16),
            pltpu.VMEM((MODEL, QA), BF16),
            pltpu.VMEM((MODEL, CA), BF16),
            pltpu.VMEM((MODEL, CA), BF16),
            pltpu.VMEM((TOK, CA), F32),
            pltpu.VMEM((TOK, CA), F32),
            pltpu.VMEM((TOK, 2 * KEY), BF16),
            pltpu.VMEM((TOK, 2 * KEY), BF16),
            pltpu.VMEM((TOK, 2 * VAL), BF16),
            pltpu.VMEM((TOK, 2 * KEY), F32),
            pltpu.VMEM((TOK, 2 * VAL), F32),
            pltpu.VMEM((TOK, 2 * KEY), BF16),
            pltpu.VMEM((2 * VAL, KEY), F32),
            pltpu.VMEM((8, 2 * KEY), F32),
            pltpu.VMEM((2, 2 * VAL, KEY), BF16),
            pltpu.VMEM((2, 8, 2 * KEY), F32),
            pltpu.VMEM((6, 2 * VAL, KEY), BF16),
            pltpu.VMEM((6, 8, 2 * KEY), F32),
            pltpu.VMEM((TOK + 8, 512), F32),
            dma((8,)),
            dma((4, 20)),
            dma((4, 20)),
            dma((10,)),
            dma((10,)),
            dma((2, 6)),
            dma((2, 6)),
            dma((2,)),
        ],
        compiler_params=pltpu.CompilerParams(
            collective_id=0, has_side_effects=True, vmem_limit_bytes=60 * 1024 * 1024
        ),
        name="front",
    )(*args)


CHUNKS = 8
CW = MODEL // CHUNKS


def back_kernel(
    attn,
    conv,
    w_a,
    w_c,
    out,
    mix,
    w,
    full,
    sib_send,
    sib_recv,
    far_send,
    far_recv,
    near_send,
    near_recv,
    load_sem,
    ss,
    sr,
    fs,
    fr,
    ns,
    nr,
):
    t = lax.axis_index("tp")
    core = t % 2
    xi = t // 2

    def at_x(d):
        return {"tp": ((xi + d) % 4) * 2 + core}

    to_sib = {"tp": xi * 2 + (1 - core)}
    loads = [
        pltpu.make_async_copy(attn, mix.at[:, 0:512], load_sem.at[0]),
        pltpu.make_async_copy(conv, mix.at[:, 512:1024], load_sem.at[1]),
    ]
    for c in range(CHUNKS):
        cols = pl.ds(c * CW, CW)
        loads.append(pltpu.make_async_copy(w_a.at[:, cols], w.at[c, 0:512, :], load_sem.at[2 + 2 * c]))
        loads.append(pltpu.make_async_copy(w_c.at[:, cols], w.at[c, 512:1024, :], load_sem.at[3 + 2 * c]))
    for c in loads:
        c.start()
    barrier = pltpu.get_barrier_semaphore()
    peers = [at_x(1), at_x(3), to_sib]
    for p in peers:
        pl.semaphore_signal(barrier, inc=1, device_id=p, device_id_type=MESH)
    loads[0].wait()
    loads[1].wait()
    pl.semaphore_wait(barrier, len(peers))

    def sib_copy(c):
        return pltpu.make_async_remote_copy(
            src_ref=sib_send.at[c],
            dst_ref=sib_recv.at[c],
            send_sem=ss.at[c],
            recv_sem=sr.at[c],
            device_id=to_sib,
            device_id_type=MESH,
        )

    def far_copy(c, side):
        return pltpu.make_async_remote_copy(
            src_ref=far_send.at[c, side],
            dst_ref=far_recv.at[c, side],
            send_sem=fs.at[c, side],
            recv_sem=fr.at[c, side],
            device_id=at_x(1 if side == 0 else 3),
            device_id_type=MESH,
        )

    def near_copy(c, side):
        return pltpu.make_async_remote_copy(
            src_ref=near_send.at[c, side],
            dst_ref=near_recv.at[c, side],
            send_sem=ns.at[c, side],
            recv_sem=nr.at[c, side],
            device_id=at_x(1 if side == 0 else 3),
            device_id_type=MESH,
        )

    def group(d, mine):
        g = ((xi + d) % 4) * 2 + (core if mine else 1 - core)
        return pl.multiple_of(g * ROWS, 32)

    def stage_a(c):
        loads[2 + 2 * c].wait()
        loads[3 + 2 * c].wait()

        def tile(i, _):
            r = pl.ds(pl.multiple_of((i % 3) * 256, 256), 256)
            k = pl.ds(pl.multiple_of((i // 3) * 256, 256), 256)
            full[c % 4, r, k] = mm(mix[r, :], w[c, :, k])
            return 0

        lax.fori_loop(0, 3 * (CW // 256), tile, 0)
        for d in range(4):
            sib_send[c, d * ROWS : (d + 1) * ROWS, :] = full[c % 4, pl.ds(group(d, False), ROWS), :].astype(BF16)
        sib_copy(c).start()

    def pair(c, d, r0, rows):
        here = full[c % 4, pl.ds(pl.multiple_of(group(d, True) + r0, 16), rows), :]
        return here + sib_recv[c, d * ROWS + r0 : d * ROWS + r0 + rows, :].astype(F32)

    def stage_b(c):
        sib_copy(c).wait_recv()
        far_send[c, 0] = pair(c, 2, 0, 48).astype(BF16)
        far_send[c, 1] = pair(c, 2, 48, 48).astype(BF16)
        far_copy(c, 0).start()
        far_copy(c, 1).start()

    def stage_c(c):
        far_copy(c, 0).wait_recv()
        near_send[c, 0, 0:48, :] = (pair(c, 1, 0, 48) + far_recv[c, 0].astype(F32)).astype(BF16)
        near_send[c, 0, 48:96, :] = pair(c, 1, 48, 48).astype(BF16)
        near_copy(c, 0).start()
        far_copy(c, 1).wait_recv()
        near_send[c, 1, 0:48, :] = pair(c, 3, 0, 48).astype(BF16)
        near_send[c, 1, 48:96, :] = (pair(c, 3, 48, 48) + far_recv[c, 1].astype(F32)).astype(BF16)
        near_copy(c, 1).start()

    def stage_d(c):
        near_copy(c, 0).wait_recv()
        near_copy(c, 1).wait_recv()
        total = pair(c, 0, 0, ROWS) + near_recv[c, 0].astype(F32) + near_recv[c, 1].astype(F32)
        out[:, c * CW : (c + 1) * CW] = total.astype(BF16)

    for i in range(CHUNKS + 3):
        if i < CHUNKS:
            stage_a(i)
        if 0 <= i - 1 < CHUNKS:
            stage_b(i - 1)
        if 0 <= i - 2 < CHUNKS:
            stage_c(i - 2)
        if 0 <= i - 3 < CHUNKS:
            stage_d(i - 3)
    for c in range(CHUNKS):
        sib_copy(c).wait_send()
        for side in (0, 1):
            far_copy(c, side).wait_send()
            near_copy(c, side).wait_send()


def back(*args):
    any_ = pl.BlockSpec(memory_space=pl.ANY)
    vmem = pl.BlockSpec(memory_space=pltpu.VMEM)
    dma = pltpu.SemaphoreType.DMA
    return pl.pallas_call(
        back_kernel,
        out_shape=jax.ShapeDtypeStruct((ROWS, MODEL), BF16),
        in_specs=[any_] * 4,
        out_specs=vmem,
        scratch_shapes=[
            pltpu.VMEM((TOK, 1024), BF16),
            pltpu.VMEM((CHUNKS, 1024, CW), BF16),
            pltpu.VMEM((4, TOK, CW), F32),
            pltpu.VMEM((CHUNKS, 4 * ROWS, CW), BF16),
            pltpu.VMEM((CHUNKS, 4 * ROWS, CW), BF16),
            pltpu.VMEM((CHUNKS, 2, 48, CW), BF16),
            pltpu.VMEM((CHUNKS, 2, 48, CW), BF16),
            pltpu.VMEM((CHUNKS, 2, ROWS, CW), BF16),
            pltpu.VMEM((CHUNKS, 2, ROWS, CW), BF16),
            dma((2 + 2 * CHUNKS,)),
            dma((CHUNKS,)),
            dma((CHUNKS,)),
            dma((CHUNKS, 2)),
            dma((CHUNKS, 2)),
            dma((CHUNKS, 2)),
            dma((CHUNKS, 2)),
        ],
        compiler_params=pltpu.CompilerParams(
            collective_id=1, has_side_effects=True, vmem_limit_bytes=60 * 1024 * 1024
        ),
        name="back",
    )(*args)


def body(
    hidden_activations,
    entry_rescale_vector,
    probe_matrix,
    lookup_address_matrix,
    payload_matrix,
    postfilter_switch_matrix,
    prefilter_switch_matrix,
    filter_source_matrix,
    forget_left_factor,
    forget_right_factor,
    forget_offset_per_feature,
    forget_spike_additions,
    subspace_rescale_vector,
    depthwise_filter_taps,
    mixer_result_matrix,
    filter_result_matrix,
):
    spikes = jnp.repeat(jnp.transpose(forget_spike_additions), KEY, axis=1)
    mixed_attn, mixed_conv = front(
        hidden_activations,
        entry_rescale_vector.astype(F32)[None, :],
        probe_matrix,
        lookup_address_matrix,
        payload_matrix,
        postfilter_switch_matrix,
        prefilter_switch_matrix,
        filter_source_matrix,
        forget_left_factor,
        forget_right_factor,
        forget_offset_per_feature[None, :],
        spikes,
        subspace_rescale_vector.astype(F32),
        depthwise_filter_taps.astype(F32),
    )
    return back(mixed_attn, mixed_conv, mixer_result_matrix, filter_result_matrix)


def solution(mesh):
    split = Mesh(mesh.devices.reshape(4, 4, mesh.shape["tp"]), ("sp_0", "sp_1", "tp"))
    in_specs = (
        P(SP_TP, None),
        P(),
        P(SP, "tp"),
        P(SP, "tp"),
        P(SP, "tp"),
        P(SP, "tp"),
        P(SP, "tp"),
        P(SP, "tp"),
        P(),
        P(None, "tp"),
        P("tp"),
        P("tp", SP),
        P("tp", None),
        P(None, "tp"),
        P("tp", None),
        P("tp", None),
    )
    out_specs = P(SP_TP, None)
    return jax.shard_map(body, mesh=split, in_specs=in_specs, out_specs=out_specs, check_vma=False)
```

time: 312 us -> 196 us (0.63)
  Pallas kernels: 0 us -> 184 us
  waiting for transfers between devices: 128 us -> 0 us
  matrix products: 72.9 us -> 0 us
  blocking collectives: 45.9 us -> 0 us
  other arithmetic: 40.2 us -> 3.83 us
  between operations: 13.5 us -> 0.04 us
  starting transfers between devices: 3.27 us -> 0 us
    pallas_call x0 -> x2, Pallas kernels: none -> 184 us  [the longest x1 143 us: front(): pl.pallas_call(front_kernel, out_shape=(jax.ShapeDtypeStruct((TOK, 2 * VA...]
    all_gather x3 -> x0, waiting for transfers between devices: 84.3 us -> none  [the longest x2 42.6 us: in_one_piece(): lax.all_gather(both, axis, axis=dim, tiled=True)]
    dot_general x13 -> x0, matrix products: 72.9 us -> none  [the longest x5 32.9 us: accumulate(): jnp.dot(normalized_input, rows_now, preferred_element_type=jnp.float32)]
    all_gather x4 -> x0, blocking collectives: 45.9 us -> none  [entering(): lax.all_gather(part.astype(kind), axis)]
    reduce_scatter x1 -> x0, waiting for transfers between devices: 43 us -> none  [body(): lax.psum_scatter((jnp.dot(mixed_attn, mixer_result_matrix, preferred_elem...]
    add x12 -> x0, other arithmetic: 12.9 us -> none  [advance(): return (jnp.exp(decay_now)[..., None] * state + update_now, state)]
    dynamic_update_slice x12 -> x0, other arithmetic: 8.77 us -> none  [block_terms(): final_state, state_in = lax.scan(advance, start_state, (block_end, updates))]
    reduce_sum x2 -> x0, other arithmetic: 4.24 us -> none  [the longest x1 4.22 us: norm_values(): meansq = jnp.mean(rows_f * rows_f, axis=-1, keepdims=True)]
  transfers between devices with their start and end apart: 5 -> 0, of which waited for: 4 -> 0; matrix products, arithmetic and copies ran while one was open for 29% -> 0% of each run, Pallas kernels for 0% -> 0%
where the time goes in v1:
time: 196 us; the launch traced here: 195 us
  Pallas kernels  184 us (94%)
  local copies, waits for them, and re-layouts  7.2 us (4%)
  other arithmetic  3.83 us (2%)
    pallas_call x1, Pallas kernels, front(): pl.pallas_call(front_kernel, out_shape=(jax.ShapeDtypeStruct((TOK, 2 * VA...  143 us
    pallas_call x1, Pallas kernels, back(): pl.pallas_call(back_kernel, out_shape=jax.ShapeDtypeStruct((ROWS, MODEL),...  41.1 us
    unnamed x3, local copies, waits for them, and re-layouts  5.37 us

profile of v1, /device:TPU:1, one launch (start us, length us, event | category | flops | bytes accessed | tf_op | source)
XLA Modules:
  0.0 195.0 jit_solution(14001496609139984640)
XLA Ops:
  0.0 1.3 convert_element_type.7.head_gain
  1.3 1.3 convert_element_type.8.taps
  2.5 1.3 broadcast_in_dim.15
  3.8 0.9 copy.17
  4.7 1.0 broadcast_in_dim.14
  5.7 0.9 copy.21
  6.6 2.4 %copy.18.left = bf16[4096,64]{1,0:T(8,128)(2,1)} copy(bf16[4096,64]{0,1:T(8,128)(2,1)} %param.24) | data formatting | bytes 1048576 | tf_op args[8]
  9.0 142.9 %front.1 = (bf16[768,512]{1,0:T(8,128)(2,1)}, bf16[768,512]{1,0:T(8,128)(2,1)}) custom-call(bf16[96,4096]{1,0:T(8,128)(2,1)} %x_in.1, f32[1,4096]{1,0:T(1,128)} %bitcast.9, bf16[256,256]{1,0:T(8,128)(2,1)} %w_q.1, bf16[256,256]{1,0:T(8,128)(2,1)} %w_k.1, bf16[256,512]{1,0:T(8,128)(2,1)} %w_v.1, bf16[256,512]{1,0:T(8,128)(2,1)} %w_out.1, ...), custom_call_target="tpu_custom_call" | custom-call | tf_op jit(solution)/shard_map/front/pallas_call | solution.py:502
  151.9 41.1 %back.1 = bf16[96,4096]{1,0:T(8,128)(2,1)} custom-call(bf16[768,512]{1,0:T(8,128)(2,1)} %get-tuple-element.7.attn, bf16[768,512]{1,0:T(8,128)(2,1)} %get-tuple-element.8.conv, bf16[512,4096]{1,0:T(8,128)(2,1)} %w_a.1, bf16[512,4096]{1,0:T(8,128)(2,1)} %w_c.1), custom_call_target="tpu_custom_call" | custom-call | tf_op jit(solution)/shard_map/back/pallas_call | solution.py:696
  193.0 2.1 %copy.23 = bf16[96,4096]{1,0:T(8,128)(2,1)} copy(bf16[96,4096]{1,0:T(8,128)(2,1)} %back.1) | data formatting | bytes 1572864

commit v2 on v0

v2 whole, which is shorter than its diff:
```python
import jax
import jax.numpy as jnp
from jax import lax
from jax.experimental import pallas as pl
from jax.experimental.pallas import tpu as pltpu
from jax.sharding import Mesh
from jax.sharding import PartitionSpec as P

MESH = pl.DeviceIdType.MESH
SP = ("sp_0", "sp_1")
SP_TP = ("sp_0", "sp_1", "tp")
F32 = jnp.float32
BF16 = jnp.bfloat16
HIGHEST = lax.Precision.HIGHEST

BLOCK = 64
ROWS = 96
TOK = 768
MODEL = 4096
KB = 256
LATE = 128
EARLY = 512 - LATE
MIX = 512 + EARLY
CHUNKS = 8
CW = MODEL // CHUNKS
KEY, VAL = 128, 256
EPS = 1e-06
DELTA = (0, 3, 1, 2)


def nt(a, b):
    return lax.dot_general(a, b, (((1,), (1,)), ((), ())), preferred_element_type=F32)


def tn(a, b):
    return lax.dot_general(a, b, (((0,), (0,)), ((), ())), preferred_element_type=F32)


def mm(a, b):
    return jnp.dot(a, b, preferred_element_type=F32)


def plan(p):
    p.first("q")
    p.ring_start("x")
    p.second("q", 0)
    p.wfirst("q")
    p.second("q", 1)
    p.ring_relay("x")
    p.wfh("q")
    p.second("q", 2)
    p.second("q", 3)
    p.wsecond("q", 0)
    p.ring_mid("x")
    p.ring_start("f")
    p.wsecond("q", 1)
    p.ring_far("x")
    p.wsecond("q", 2)
    p.first("c")
    p.wsecond("q", 3)
    p.ring_end("x")
    p.rates()
    p.second("c", 0)
    p.wsh("q", 0)
    p.project("q", 0)
    p.wsh("q", 1)
    p.project("q", 1)
    p.wfirst("c")
    p.second("c", 1)
    p.wsh("q", 2)
    p.project("q", 2)
    p.wsh("q", 3)
    p.project("q", 3)
    p.key_state()
    p.state(0)
    p.ring_relay("f")
    p.wfh("c")
    p.wsecond("c", 0)
    p.second("c", 2)
    p.attend(0, 6)
    p.rstate(0)
    p.second("c", 3)
    p.wsecond("c", 1)
    p.ring_mid("f")
    p.attend(6, 12)
    p.wstate(0)
    p.fold_y()
    p.state(1)
    p.load_out()
    p.wsh("c", 0)
    p.project("c", 0)
    p.wsecond("c", 2)
    p.rstate(1)
    p.wsecond("c", 3)
    p.wsh("c", 1)
    p.project("c", 1)
    p.first("d")
    p.ring_far("f")
    p.wstate(1)
    p.fold_z()
    p.second("d", 0)
    p.wsh("c", 2)
    p.project("c", 2)
    p.wfirst("d")
    p.second("d", 1)
    p.second("d", 2)
    p.wsh("c", 3)
    p.project("c", 3)
    p.wfh("d")
    p.second("d", 3)
    p.conv("c")

    def late(k):
        p.wsh("d", k)
        p.project("d", k)

    def finish_late():
        p.conv("d")
        p.exchange()

    extra = {
        0: lambda: p.wsecond("d", 0),
        1: lambda: p.wsecond("d", 1),
        2: lambda: (p.wsecond("d", 2), p.wsecond("d", 3)),
        3: lambda: late(0),
        4: lambda: late(1),
        5: lambda: late(2),
        6: lambda: (late(3), finish_late()),
        8: lambda: p.ring_end("f"),
    }
    for i in range(CHUNKS + 3):
        if i < CHUNKS:
            p.pair_products(i)
        if 0 <= i - 1 < CHUNKS:
            p.far(i - 1)
        if 0 <= i - 2 < CHUNKS:
            p.near(i - 2)
        if i in extra:
            extra[i]()
        if 0 <= i - 3 < CHUNKS:
            p.gather(i - 3)
    p.last()


def layer_kernel(
    x_in,
    gain,
    w_q,
    w_k,
    w_v,
    w_out,
    w_in,
    w_src,
    left,
    right,
    offset,
    spikes,
    head_gain,
    taps,
    w_a,
    w_c,
    out,
    xs,
    qa,
    qb,
    ca,
    cb,
    da,
    db,
    wf,
    acc_a,
    acc_b,
    acc_da,
    acc_db,
    qrows,
    krows,
    vrows,
    within,
    tail,
    spk,
    inside,
    q_far,
    state,
    prefix,
    st_send,
    dec_send,
    st_recv,
    dec_recv,
    gated_c,
    gated_d,
    mix,
    late_mix,
    late_recv,
    own,
    sib_send,
    sib_recv,
    far_send,
    far_recv,
    near_send,
    near_recv,
    load_sem,
    out_sem,
    w_send,
    w_recv,
    x_send,
    x_recv,
    s_send,
    s_recv,
    h_send,
    h_recv,
    e_send,
    e_recv,
    ss,
    sr,
    fs,
    fr,
    ns,
    nr,
):
    z = lax.axis_index("sp_0")
    y = lax.axis_index("sp_1")
    t = lax.axis_index("tp")
    core = t % 2
    xi = t // 2
    sp = z * 4 + y
    sp_next = (sp + 1) % 16
    sp_prev = (sp + 15) % 16
    to_next = {"sp_0": sp_next // 4, "sp_1": sp_next % 4}
    to_prev = {"sp_0": sp_prev // 4, "sp_1": sp_prev % 4}
    to_sib = {"tp": xi * 2 + (1 - core)}

    def at_z(d):
        return {"sp_0": (z + d) % 4}

    def at_y(d):
        return {"sp_1": (y + d) % 4}

    def at_x(d):
        return {"tp": ((xi + d) % 4) * 2 + core}

    def remote(ref, dst, sems, at, to):
        return pltpu.make_async_remote_copy(
            src_ref=ref,
            dst_ref=dst,
            send_sem=sems[0].at[at],
            recv_sem=sems[1].at[at],
            device_id=to,
            device_id_type=MESH,
        )

    own0 = pl.ds(pl.multiple_of(sp * KB, KB), KB)
    own1 = pl.ds(pl.multiple_of((y * 4 + z) * KB, KB), KB)
    own_rows = pl.multiple_of(t * ROWS, 32)
    loads = [
        (x_in, xs.at[pl.ds(own_rows, ROWS), :]),
        (w_q, qa.at[own0, 0:256]),
        (w_k, qa.at[own0, 256:512]),
        (w_v, qb.at[own1, :]),
        (w_in.at[:, 256:384], ca.at[own0, 0:128]),
        (w_src.at[:, 0:384], ca.at[own0, 128:512]),
        (w_out.at[:, 0:384], cb.at[own1, 0:384]),
        (w_in.at[:, 0:256], cb.at[own1, 384:640]),
        (w_in.at[:, 384:512], da.at[own0, 0:128]),
        (w_src.at[:, 384:512], da.at[own0, 128:256]),
        (w_out.at[:, 384:512], db.at[own1, :]),
        (w_c.at[EARLY:512, :], wf.at[pl.ds(pl.multiple_of(t * LATE, LATE), LATE), :]),
    ]
    loads = [pltpu.make_async_copy(a, b, load_sem.at[i]) for i, (a, b) in enumerate(loads)]
    for c in loads:
        c.start()

    barrier = pltpu.get_barrier_semaphore()
    peers = [at_z(1), at_z(3), at_y(1), at_y(3), to_next, to_prev] + [{"tp": (t + d) % 8} for d in range(1, 8)]
    for p in peers:
        pl.semaphore_signal(barrier, inc=1, device_id=p, device_id_type=MESH)

    loads[0].wait()

    def norm_rows(i, _):
        r = pl.ds(pl.multiple_of(own_rows + i * 16, 16), 16)
        v = xs[r, :].astype(F32)
        inv = lax.rsqrt(jnp.mean(v * v, axis=-1, keepdims=True) + EPS)
        g = gain[...].astype(F32)
        for c in range(32):
            k = slice(c * 128, (c + 1) * 128)
            xs[r, k] = (v[:, k] * inv * g[c : c + 1, :]).astype(BF16)
        return 0

    lax.fori_loop(0, ROWS // 16, norm_rows, 0)
    spk[...] = jnp.zeros_like(spk)
    spk[0:2, :] = spikes[...]
    for c in loads[1:]:
        c.wait()
    pl.semaphore_wait(barrier, len(peers))

    started = []
    started_q = []

    def go(c, group=None):
        c.start()
        (started_q if group == "q" else started).append(c)

    bufs = {"q": (qa, qb), "c": (ca, cb), "d": (da, db)}
    accs = {"q": (acc_a, acc_b.at[:, 0:512]), "c": (acc_a, acc_b), "d": (acc_da, acc_db)}
    base = {"q": 0, "c": 2, "d": 4}
    rings = {"x": (xs, ROWS, 0), "f": (wf, LATE, 10)}
    xm, xp, xf = (xi + 3) % 4, (xi + 1) % 4, (xi + 2) % 4

    def w_copy(g, path, slot, du, dv, axis, step, row=0, rows=KB):
        u0, v0 = (z, y) if path == 0 else (y, z)
        j = ((u0 + du) % 4) * 4 + (v0 + dv) % 4
        ref = bufs[g][path].at[pl.ds(pl.multiple_of(j * KB + row, 128), rows), :]
        to = at_z(step) if (axis == 0) == (path == 0) else at_y(step)
        return remote(ref, ref, (w_send, w_recv), (base[g] + path, slot), to)

    def ring_copy(n, slot, x_from, top, halves, to, c=None):
        buf, rows, first = rings[n]
        half = rows // 2
        at = (x_from * 2 + (core if c is None else c)) * rows + (0 if top else half)
        ref = buf.at[pl.ds(pl.multiple_of(at, 16), half * halves), :]
        return remote(ref, ref, (x_send, x_recv), first + slot, to)

    right_x, left_x = at_x(1), at_x(3)

    def st_copy(ph, slot):
        to = (at_y if ph == 0 else at_z)(1 if slot % 2 == 0 else 3)
        i = ph * 3
        if slot < 2:
            a, b = st_send.at[ph], st_recv.at[i + 2 * slot]
        else:
            half = pl.ds((slot - 2) * VAL, VAL)
            a, b = st_recv.at[i + 2 * (slot - 2), half, :], st_recv.at[i + 1, half, :]
        return remote(a, b, (s_send, s_recv), ph * 8 + slot, to)

    def dec_copy(ph, slot):
        to = (at_y if ph == 0 else at_z)(1 if slot != 1 else 3)
        i = ph * 3
        if slot < 2:
            a, b = dec_send.at[ph], dec_recv.at[i + 2 * slot]
        else:
            a, b = dec_recv.at[i], dec_recv.at[i + 1]
        return remote(a, b, (s_send, s_recv), ph * 8 + 4 + slot, to)

    def halo_copy(g):
        buf = gated_c if g == "c" else gated_d
        i = 0 if g == "c" else 1
        return remote(buf.at[pl.ds(TOK, 8), :], buf.at[pl.ds(0, 8), :], (h_send, h_recv), i, to_next)

    def sib_copy(c):
        return remote(sib_send.at[c % 2], sib_recv.at[c], (ss, sr), c, to_sib)

    def far_copy(c, side):
        return remote(far_send.at[c, side], far_recv.at[c, side], (fs, fr), (c, side), right_x if side == 0 else left_x)

    def near_copy(c, side):
        return remote(near_send.at[c, side], near_recv.at[c, side], (ns, nr), (c, side), right_x if side == 0 else left_x)

    def late_copy(d, sending):
        g = (t + d) % 8
        me = t if sending else (t + 8 - d) % 8
        src = late_mix.at[pl.ds(pl.multiple_of(g * ROWS, 32), ROWS), :]
        return remote(src, late_recv.at[me], (e_send, e_recv), d - 1, {"tp": g})

    def out_block(i):
        return (qa if i < CHUNKS // 2 else qb).at[pl.ds((i % (CHUNKS // 2)) * MIX, MIX), :]

    def out_loads(i):
        cols = pl.ds(i * CW, CW)
        w = out_block(i)
        return (
            pltpu.make_async_copy(w_a.at[:, cols], w.at[0:512, :], out_sem.at[2 * i]),
            pltpu.make_async_copy(w_c.at[0:EARLY, cols], w.at[512:MIX, :], out_sem.at[2 * i + 1]),
        )

    def head(h):
        return slice(h * KEY, (h + 1) * KEY), slice(h * VAL, (h + 1) * VAL)

    class Device:
        def first(self, g):
            for p in (0, 1):
                go(w_copy(g, p, 0, 0, 0, 0, 1), g)
                go(w_copy(g, p, 1, 0, 0, 0, 3), g)

        def wfirst(self, g):
            for p in (0, 1):
                w_copy(g, p, 0, 3, 0, 0, 1).wait_recv()
                go(w_copy(g, p, 2, 3, 0, 0, 1, 0, 128), g)
                w_copy(g, p, 1, 1, 0, 0, 3).wait_recv()
                go(w_copy(g, p, 3, 1, 0, 0, 3, 128, 128), g)

        def wfh(self, g):
            for p in (0, 1):
                w_copy(g, p, 2, 2, 0, 0, 1, 0, 128).wait_recv()
                w_copy(g, p, 3, 2, 0, 0, 3, 128, 128).wait_recv()

        def second(self, g, k):
            for p in (0, 1):
                go(w_copy(g, p, 4 + 2 * k, DELTA[k], 0, 1, 1), g)
                go(w_copy(g, p, 5 + 2 * k, DELTA[k], 0, 1, 3), g)

        def wsecond(self, g, k):
            for p in (0, 1):
                w_copy(g, p, 4 + 2 * k, DELTA[k], 3, 1, 1).wait_recv()
                go(w_copy(g, p, 12 + 2 * k, DELTA[k], 3, 1, 1, 0, 128), g)
                w_copy(g, p, 5 + 2 * k, DELTA[k], 1, 1, 3).wait_recv()
                go(w_copy(g, p, 13 + 2 * k, DELTA[k], 1, 1, 3, 128, 128), g)

        def wsh(self, g, k):
            for p in (0, 1):
                w_copy(g, p, 12 + 2 * k, DELTA[k], 2, 1, 1, 0, 128).wait_recv()
                w_copy(g, p, 13 + 2 * k, DELTA[k], 2, 1, 3, 128, 128).wait_recv()

        def ring_start(self, n):
            go(ring_copy(n, 0, xi, True, 1, right_x))
            go(ring_copy(n, 2, xi, False, 1, left_x))
            go(ring_copy(n, 1, xi, False, 1, right_x))
            go(ring_copy(n, 3, xi, True, 1, left_x))
            go(ring_copy(n, 6, xi, True, 2, to_sib))

        def ring_relay(self, n):
            ring_copy(n, 0, xm, True, 1, right_x).wait_recv()
            go(ring_copy(n, 4, xm, True, 1, right_x))
            ring_copy(n, 2, xp, False, 1, left_x).wait_recv()
            go(ring_copy(n, 5, xp, False, 1, left_x))

        def ring_mid(self, n):
            ring_copy(n, 1, xm, False, 1, right_x).wait_recv()
            go(ring_copy(n, 7, xm, True, 2, to_sib))
            ring_copy(n, 3, xp, True, 1, left_x).wait_recv()
            go(ring_copy(n, 8, xp, True, 2, to_sib))

        def ring_far(self, n):
            ring_copy(n, 4, xf, True, 1, right_x).wait_recv()
            ring_copy(n, 5, xf, False, 1, left_x).wait_recv()
            go(ring_copy(n, 9, xf, True, 2, to_sib))

        def ring_end(self, n):
            for slot, src in ((6, xi), (7, xm), (8, xp), (9, xf)):
                ring_copy(n, slot, src, True, 2, to_sib, 1 - core).wait_recv()

        def rates(self):
            lane_head = lax.broadcasted_iota(jnp.int32, (8, 2 * KEY), 1) // KEY
            pick = jnp.where(lax.broadcasted_iota(jnp.int32, (8, 2 * KEY), 0) == lane_head, 1.0, 0.0).astype(F32)
            row = lax.broadcasted_iota(jnp.int32, (128, 128), 0)
            col = lax.broadcasted_iota(jnp.int32, (128, 128), 1)
            low_tri = jnp.where((row >= col) & (row // BLOCK == col // BLOCK), 1.0, 0.0).astype(F32)

            def step(i, _):
                r = pl.ds(pl.multiple_of(i * 128, 128), 128)
                low = nt(xs[r, :], left[...]).astype(BF16)
                g = mm(low, right[...]) + offset[...]
                ls = jnp.minimum(g, 0.0) - jnp.log1p(jnp.exp(-jnp.abs(g)))
                spike = lax.dot_general(
                    spk[:, r], pick, (((0,), (0,)), ((), ())), precision=HIGHEST, preferred_element_type=F32
                )
                within[r, :] = jnp.dot(
                    low_tri, ls * (1.0 / 16.0) + spike, precision=HIGHEST, preferred_element_type=F32
                )
                return 0

            lax.fori_loop(0, TOK // 128, step, 0)
            prefix[0:1, :] = jnp.zeros((1, 2 * KEY), F32)

            def back(i, _):
                n = TOK // BLOCK - 1 - i
                w = within[pl.ds(pl.multiple_of(n * BLOCK, BLOCK), BLOCK), :]
                end = w[BLOCK - 1 : BLOCK, :]
                later = prefix[0:1, :]
                tail[pl.ds(pl.multiple_of(n * BLOCK, BLOCK), BLOCK), :] = jnp.exp(end - w + later)
                prefix[0:1, :] = later + end
                return 0

            lax.fori_loop(0, TOK // BLOCK, back, 0)
            dec_send[0] = jnp.broadcast_to(jnp.exp(prefix[0:1, :]), (8, 2 * KEY))

        def project(self, g, k):
            for p in (0, 1):
                w, acc = bufs[g][p], accs[g][p]
                u = ((z if p == 0 else y) + DELTA[k]) % 4
                if p == 0:
                    lhs = xs[:, pl.ds(pl.multiple_of(u * 1024, 1024), 1024)]
                else:
                    lhs = jnp.concatenate(
                        [xs[:, pl.ds(pl.multiple_of((v * 4 + u) * KB, KB), KB)] for v in range(4)], axis=1
                    )
                part = mm(lhs, w[pl.ds(pl.multiple_of(u * 1024, 1024), 1024), :])
                if k == 0:
                    acc[...] = part
                else:
                    acc[...] += part

        def key_state(self):
            def step(i, _):
                r = pl.ds(pl.multiple_of(i * 64, 64), 64)
                qrows[r, :] = acc_a[r, 0:256].astype(BF16)
                krows[r, :] = acc_a[r, 256:512].astype(BF16)
                vrows[r, :] = acc_b[r, 0:512].astype(BF16)
                return 0

            lax.fori_loop(0, TOK // 64, step, 0)
            k_tail = (krows[...].astype(F32) * tail[...]).astype(BF16)
            for h in range(2):
                kc, vc = head(h)
                s = tn(vrows[:, vc], k_tail[:, kc])
                st_send[0, vc, :] = s.astype(BF16)
            state[...] = jnp.zeros_like(state)
            prefix[0:1, :] = jnp.zeros((1, 2 * KEY), F32)

        def state(self, ph):
            for slot in (0, 1):
                go(st_copy(ph, slot))
                go(dec_copy(ph, slot))

        def rstate(self, ph):
            for slot in (0, 1):
                st_copy(ph, slot).wait_recv()
                dec_copy(ph, slot).wait_recv()
                go(st_copy(ph, slot + 2))
            go(dec_copy(ph, 2))

        def wstate(self, ph):
            st_copy(ph, 2).wait_recv()
            st_copy(ph, 3).wait_recv()
            dec_copy(ph, 2).wait_recv()

        def attend(self, lo, hi):
            def step(n, _):
                r = pl.ds(pl.multiple_of(n * BLOCK, BLOCK), BLOCK)
                row = lax.broadcasted_iota(jnp.int32, (BLOCK, BLOCK), 0)
                col = lax.broadcasted_iota(jnp.int32, (BLOCK, BLOCK), 1)
                causal = row >= col
                w = within[r, :]
                end = w[BLOCK - 1 : BLOCK, :]
                mid = end * 0.5
                q_s = qrows[r, :].astype(F32) * (KEY**-0.5) * jnp.exp(w - mid)
                k_s = krows[r, :].astype(F32) * jnp.exp(mid - w)
                e_mid = jnp.exp(mid)
                q_d = q_s * e_mid
                k_t = (k_s * e_mid).astype(BF16)
                e_end = jnp.exp(end)
                before = prefix[0:1, :]
                q_far[r, :] = (q_d * jnp.exp(before)).astype(BF16)
                prefix[0:1, :] = before + end
                q_d = q_d.astype(BF16)
                q_s = q_s.astype(BF16)
                k_s = k_s.astype(BF16)
                for h in range(2):
                    kc, vc = head(h)
                    v = vrows[r, vc]
                    scores = jnp.where(causal, nt(q_s[:, kc], k_s[:, kc]), 0.0).astype(BF16)
                    s = state[vc, :]
                    inside[r, vc] = mm(scores, v) + nt(q_d[:, kc], s.astype(BF16))
                    state[vc, :] = s * e_end[:, kc] + tn(v, k_t[:, kc])
                return 0

            lax.fori_loop(lo, hi, step, 0)

        def fold(self, total, decay, i, use):
            dec = jnp.where(use, dec_recv[i][0:1, :], 1.0)
            out_ = []
            for h in range(2):
                kc, vc = head(h)
                got = jnp.where(use, st_recv[i, vc, :].astype(F32), 0.0)
                out_.append(total[h] * dec[:, kc] + got)
            return out_, decay * dec

        def fold_y(self):
            own_decay = dec_send[0][0:1, :]
            total = [jnp.zeros((VAL, KEY), F32) for _ in range(2)]
            decay = jnp.ones((1, 2 * KEY), F32)
            for d in (3, 2, 1):
                total, decay = self.fold(total, decay, d - 1, d <= y)
            prefix[1:2, :] = decay
            for h in range(2):
                kc, vc = head(h)
                state[vc, :] = total[h]
                total[h] = total[h] * own_decay[:, kc] + st_send[0, vc, :].astype(F32)
            decay = decay * own_decay
            for d in (3, 2, 1):
                total, decay = self.fold(total, decay, d - 1, d > y)
            for h in range(2):
                kc, vc = head(h)
                st_send[1, vc, :] = total[h].astype(BF16)
            dec_send[1] = jnp.broadcast_to(decay, (8, 2 * KEY))

        def fold_z(self):
            total = [jnp.zeros((VAL, KEY), F32) for _ in range(2)]
            decay = jnp.ones((1, 2 * KEY), F32)
            for d in (3, 2, 1):
                total, decay = self.fold(total, decay, 3 + d - 1, d <= z)
            decay = prefix[1:2, :]
            for h in range(2):
                kc, vc = head(h)
                state[vc, :] = total[h] * decay[:, kc] + state[vc, :]
            hg = head_gain[...].astype(F32)

            def finish(g, _):
                r = pl.ds(pl.multiple_of(g * ROWS, 32), ROWS)
                to = self.place(g)
                for h in range(2):
                    kc, vc = head(h)
                    a = inside[r, vc] + nt(q_far[r, kc], state[vc, :].astype(BF16))
                    ms = jnp.mean(a * a, axis=-1, keepdims=True)
                    mix[to, vc] = (a * lax.rsqrt(ms + EPS) * hg[h : h + 1, :]).astype(BF16)
                return 0

            lax.fori_loop(0, 8, finish, 0)

        def place(self, g):
            mine = 1 - (g + core) % 2
            d = (g // 2 + 4 - xi) % 4
            return pl.ds(pl.multiple_of((mine * 4 + d) * ROWS, 32), ROWS)

        def conv(self, g):
            gated = gated_c if g == "c" else gated_d
            lanes = slice(0, EARLY) if g == "c" else slice(EARLY, 512)

            def rnd(v):
                return v.astype(BF16).astype(F32)

            def gate(i, _):
                r = pl.ds(pl.multiple_of(i * 64, 64), 64)
                o = pl.ds(pl.multiple_of(i * 64 + 8, 8), 64)
                if g == "c":
                    gated[o, 0:256] = rnd(rnd(acc_b[r, 384:640]) * rnd(acc_a[r, 128:384]))
                    gated[o, 256:384] = rnd(rnd(acc_a[r, 0:128]) * rnd(acc_a[r, 384:512]))
                else:
                    gated[o, :] = rnd(rnd(acc_da[r, 0:128]) * rnd(acc_da[r, 128:256]))
                return 0

            lax.fori_loop(0, TOK // 64, gate, 0)
            go(halo_copy(g))
            tp = taps[...].astype(F32)[:, lanes]

            def rows(i, first):
                block = gated[pl.ds(pl.multiple_of(i * ROWS, 32), ROWS + 8), :]
                if first:
                    keep = jnp.where(sp == 0, 0.0, 1.0)
                    rim = lax.broadcasted_iota(jnp.int32, (ROWS + 8, 1), 0) < 8
                    block = jnp.where(rim, block * keep, block)
                one = pltpu.roll(block, 1, 0)[8:, :]
                two = pltpu.roll(block, 2, 0)[8:, :]
                s = tp[0:1, :] * two + tp[1:2, :] * one + tp[2:3, :] * block[8:, :]
                r = pl.ds(pl.multiple_of(i * ROWS, 32), ROWS)
                if g == "c":
                    mix[self.place(i), 512:MIX] = (s * rnd(acc_b[r, 0:384])).astype(BF16)
                else:
                    late_mix[r, :] = (s * rnd(acc_db[r, :])).astype(BF16)

            def step(i, _):
                rows(i, False)
                return 0

            lax.fori_loop(1, 8, step, 0)
            halo_copy(g).wait_recv()
            rows(0, True)

        def load_out(self):
            for c in started_q:
                c.wait_send()
            for i in range(CHUNKS):
                for c in out_loads(i):
                    c.start()

        def pair_products(self, i):
            for c in out_loads(i):
                c.wait()
            w = out_block(i)
            if i >= 2:
                sib_copy(i - 2).wait_send()
            sib_send[i % 2] = mm(mix[0 : 4 * ROWS, :], w[...]).astype(BF16)
            sib_copy(i).start()
            own[i % 4] = mm(mix[4 * ROWS : TOK, :], w[...])

        def pair(self, c, d, r0, rows):
            at = slice(d * ROWS + r0, d * ROWS + r0 + rows)
            return own[c % 4, at, :] + sib_recv[c, at, :].astype(F32)

        def far(self, c):
            sib_copy(c).wait_recv()
            for side in (0, 1):
                far_send[c, side] = self.pair(c, 2, side * 48, 48).astype(BF16)
                go(far_copy(c, side))

        def near(self, c):
            far_copy(c, 0).wait_recv()
            near_send[c, 0, 0:48, :] = (self.pair(c, 1, 0, 48) + far_recv[c, 0].astype(F32)).astype(BF16)
            near_send[c, 0, 48:96, :] = self.pair(c, 1, 48, 48).astype(BF16)
            go(near_copy(c, 0))
            far_copy(c, 1).wait_recv()
            near_send[c, 1, 0:48, :] = self.pair(c, 3, 0, 48).astype(BF16)
            near_send[c, 1, 48:96, :] = (self.pair(c, 3, 48, 48) + far_recv[c, 1].astype(F32)).astype(BF16)
            go(near_copy(c, 1))

        def gather(self, c):
            near_copy(c, 0).wait_recv()
            near_copy(c, 1).wait_recv()
            total = self.pair(c, 0, 0, ROWS) + near_recv[c, 0].astype(F32) + near_recv[c, 1].astype(F32)
            inside[c * ROWS : (c + 1) * ROWS, :] = total

        def exchange(self):
            for d in (1, 7, 2, 6, 3, 5, 4):
                go(late_copy(d, True))
            late_recv[t] = late_mix[pl.ds(own_rows, ROWS), :]

        def last(self):
            for d in range(1, 8):
                late_copy(d, False).wait_recv()
            lhs = jnp.concatenate([late_recv[g] for g in range(8)], axis=1)
            for i in range(CHUNKS):
                k = slice(i * CW, (i + 1) * CW)
                out[:, k] = (inside[i * ROWS : (i + 1) * ROWS, :] + mm(lhs, wf[:, k])).astype(BF16)
            for i in range(CHUNKS - 2, CHUNKS):
                sib_copy(i).wait_send()
            for c in started:
                c.wait_send()

    plan(Device())


def layer(*args):
    any_ = pl.BlockSpec(memory_space=pl.ANY)
    vmem = pl.BlockSpec(memory_space=pltpu.VMEM)
    dma = pltpu.SemaphoreType.DMA

    def f32(*shape):
        return pltpu.VMEM(shape, F32)

    def bf16(*shape):
        return pltpu.VMEM(shape, BF16)

    return pl.pallas_call(
        layer_kernel,
        out_shape=jax.ShapeDtypeStruct((ROWS, MODEL), BF16),
        in_specs=[any_, vmem] + [any_] * 6 + [vmem] * 6 + [any_] * 2,
        out_specs=vmem,
        scratch_shapes=[
            bf16(TOK, MODEL),
            bf16(MODEL, 512),
            bf16(MODEL, 512),
            bf16(MODEL, 512),
            bf16(MODEL, 640),
            bf16(MODEL, 256),
            bf16(MODEL, 128),
            bf16(8 * LATE, MODEL),
            f32(TOK, 512),
            f32(TOK, 640),
            f32(TOK, 256),
            f32(TOK, 128),
            bf16(TOK, 2 * KEY),
            bf16(TOK, 2 * KEY),
            bf16(TOK, 2 * VAL),
            f32(TOK, 2 * KEY),
            f32(TOK, 2 * KEY),
            f32(8, TOK),
            f32(TOK, 2 * VAL),
            bf16(TOK, 2 * KEY),
            f32(2 * VAL, KEY),
            f32(8, 2 * KEY),
            bf16(2, 2 * VAL, KEY),
            f32(2, 8, 2 * KEY),
            bf16(6, 2 * VAL, KEY),
            f32(6, 8, 2 * KEY),
            f32(TOK + 8, EARLY),
            f32(TOK + 8, LATE),
            bf16(TOK, MIX),
            bf16(TOK, LATE),
            bf16(8, ROWS, LATE),
            f32(4, 4 * ROWS, CW),
            bf16(2, 4 * ROWS, CW),
            bf16(CHUNKS, 4 * ROWS, CW),
            bf16(CHUNKS, 2, 48, CW),
            bf16(CHUNKS, 2, 48, CW),
            bf16(CHUNKS, 2, ROWS, CW),
            bf16(CHUNKS, 2, ROWS, CW),
            dma((12,)),
            dma((2 * CHUNKS,)),
            dma((6, 20)),
            dma((6, 20)),
            dma((20,)),
            dma((20,)),
            dma((16,)),
            dma((16,)),
            dma((2,)),
            dma((2,)),
            dma((7,)),
            dma((7,)),
            dma((CHUNKS,)),
            dma((CHUNKS,)),
            dma((CHUNKS, 2)),
            dma((CHUNKS, 2)),
            dma((CHUNKS, 2)),
            dma((CHUNKS, 2)),
        ],
        compiler_params=pltpu.CompilerParams(
            collective_id=0, has_side_effects=True, vmem_limit_bytes=67_000_000
        ),
        name="layer",
    )(*args)


def body(
    hidden_activations,
    entry_rescale_vector,
    probe_matrix,
    lookup_address_matrix,
    payload_matrix,
    postfilter_switch_matrix,
    prefilter_switch_matrix,
    filter_source_matrix,
    forget_left_factor,
    forget_right_factor,
    forget_offset_per_feature,
    forget_spike_additions,
    subspace_rescale_vector,
    depthwise_filter_taps,
    mixer_result_matrix,
    filter_result_matrix,
):
    return layer(
        hidden_activations,
        entry_rescale_vector.reshape(32, 128),
        probe_matrix,
        lookup_address_matrix,
        payload_matrix,
        postfilter_switch_matrix,
        prefilter_switch_matrix,
        filter_source_matrix,
        forget_left_factor.T,
        forget_right_factor,
        forget_offset_per_feature[None, :],
        forget_spike_additions,
        subspace_rescale_vector,
        depthwise_filter_taps,
        mixer_result_matrix,
        filter_result_matrix,
    )


def solution(mesh):
    split = Mesh(mesh.devices.reshape(4, 4, mesh.shape["tp"]), ("sp_0", "sp_1", "tp"))
    in_specs = (
        P(SP_TP, None),
        P(),
        P(SP, "tp"),
        P(SP, "tp"),
        P(SP, "tp"),
        P(SP, "tp"),
        P(SP, "tp"),
        P(SP, "tp"),
        P(),
        P(None, "tp"),
        P("tp"),
        P("tp", SP),
        P("tp", None),
        P(None, "tp"),
        P("tp", None),
        P("tp", None),
    )
    out_specs = P(SP_TP, None)
    return jax.shard_map(body, mesh=split, in_specs=in_specs, out_specs=out_specs, check_vma=False)
```

time: 312 us -> 167 us (0.54)
  Pallas kernels: 0 us -> 163 us
  waiting for transfers between devices: 128 us -> 0 us
  matrix products: 72.9 us -> 0 us
  blocking collectives: 45.9 us -> 0 us
  other arithmetic: 40.2 us -> 0 us
  between operations: 13.5 us -> 0.01 us
  local copies, waits for them, and re-layouts: 7.15 us -> 2.06 us
  starting transfers between devices: 3.27 us -> 0 us
    pallas_call x0 -> x1, Pallas kernels: none -> 163 us  [layer(): pl.pallas_call(layer_kernel, out_shape=jax.ShapeDtypeStruct((ROWS, MODEL)...]
    all_gather x3 -> x0, waiting for transfers between devices: 84.3 us -> none  [the longest x2 42.6 us: in_one_piece(): lax.all_gather(both, axis, axis=dim, tiled=True)]
    dot_general x13 -> x0, matrix products: 72.9 us -> none  [the longest x5 32.9 us: accumulate(): jnp.dot(normalized_input, rows_now, preferred_element_type=jnp.float32)]
    all_gather x4 -> x0, blocking collectives: 45.9 us -> none  [entering(): lax.all_gather(part.astype(kind), axis)]
    reduce_scatter x1 -> x0, waiting for transfers between devices: 43 us -> none  [body(): lax.psum_scatter((jnp.dot(mixed_attn, mixer_result_matrix, preferred_elem...]
    add x12 -> x0, other arithmetic: 12.9 us -> none  [advance(): return (jnp.exp(decay_now)[..., None] * state + update_now, state)]
    dynamic_update_slice x12 -> x0, other arithmetic: 8.77 us -> none  [block_terms(): final_state, state_in = lax.scan(advance, start_state, (block_end, updates))]
    convert_element_type x6 -> x0, other arithmetic: 5.65 us -> none  [the longest x1 5.42 us: row_norm(): return norm_values(rows, gain).astype(jnp.bfloat16)]
  transfers between devices with their start and end apart: 5 -> 0, of which waited for: 4 -> 0; matrix products, arithmetic and copies ran while one was open for 29% -> 0% of each run, Pallas kernels for 0% -> 0%
where the time goes in v2:
time: 167 us; the launch traced here: 165 us
  Pallas kernels  163 us (98%)
  local copies, waits for them, and re-layouts  2.06 us (1%)
    pallas_call x1, Pallas kernels, layer(): pl.pallas_call(layer_kernel, out_shape=jax.ShapeDtypeStruct((ROWS, MODEL)...  163 us

profile of v2, /device:TPU:1, one launch (start us, length us, event | category | flops | bytes accessed | tf_op | source)
XLA Modules:
  0.0 165.4 jit_solution(4966583150584612100)
XLA Ops:
  0.0 163.3 %layer.1 = bf16[96,4096]{1,0:T(8,128)(2,1)} custom-call(bf16[96,4096]{1,0:T(8,128)(2,1)} %x_in.1, bf16[32,128]{1,0:T(8,128)(2,1)} %bitcast.4, bf16[256,256]{1,0:T(8,128)(2,1)} %w_q.1, bf16[256,256]{1,0:T(8,128)(2,1)} %w_k.1, bf16[256,512]{1,0:T(8,128)(2,1)} %w_v.1, bf16[256,512]{1,0:T(8,128)(2,1)} %w_out.1, bf16[256,512]{1,0:T(8,128)(2,1)} %w_in.1, ...), custom_call_target="tpu_custom_call" | custom-call | tf_op jit(solution)/shard_map/layer/pallas_call | solution.py:732
  163.3 2.1 %copy.18 = bf16[96,4096]{1,0:T(8,128)(2,1)} copy(bf16[96,4096]{1,0:T(8,128)(2,1)} %layer.1) | data formatting | bytes 1572864

commit v3 on v2

v3 whole, which is shorter than its diff:
```python
import jax
import jax.numpy as jnp
from jax import lax
from jax.experimental import pallas as pl
from jax.experimental.pallas import tpu as pltpu
from jax.sharding import Mesh
from jax.sharding import PartitionSpec as P

MESH = pl.DeviceIdType.MESH
SP = ("sp_0", "sp_1")
SP_TP = ("sp_0", "sp_1", "tp")
F32 = jnp.float32
BF16 = jnp.bfloat16
HIGHEST = lax.Precision.HIGHEST

BLOCK = 64
ROWS = 96
TOK = 768
MODEL = 4096
KB = 256
LATE = 256
EARLY = 512 - LATE
MIX = 512 + EARLY
CHUNKS = 8
CW = MODEL // CHUNKS
KEY, VAL = 128, 256
EPS = 1e-06
DELTA = (0, 3, 1, 2)


def nt(a, b):
    return lax.dot_general(a, b, (((1,), (1,)), ((), ())), preferred_element_type=F32)


def tn(a, b):
    return lax.dot_general(a, b, (((0,), (0,)), ((), ())), preferred_element_type=F32)


def mm(a, b):
    return jnp.dot(a, b, preferred_element_type=F32)


SEND, WAIT, RUN = "send", "wait", "run"
W, R, S = "w", "r", "s"
Q, E, C, D = "q", "e", "c", "d"
X, F, H = "x", "f", "h"
T_NORM = "norm"
T_LOW_RANK = "low_rank"
T_RATE = "rate"
T_SUFFIX = "suffix"
T_PROJECT = "project"
T_KEY_STATE = "key_state"
T_ATTEND = "attend"
T_FOLD_Y = "fold_y"
T_FOLD_Z = "fold_z"
T_GATE = "gate"
T_CONV = "conv"
T_FIRST_ROWS = "first_rows"
T_EXCHANGE = "exchange"
T_LOAD_H = "load_h"
T_START_H = "start_h"
T_PAIR_PRODUCTS = "pair_products"
T_FAR = "far"
T_NEAR = "near"
T_GATHER = "gather"
T_COLLECT = "collect"
T_LAST = "last"
ORDER = (
    (SEND, W, Q, 0, 0), (SEND, W, Q, 1, 4), (SEND, W, Q, 0, 1), (SEND, W, Q, 1, 5), (SEND, W, Q, 1, 0),
    (SEND, W, Q, 0, 4), (SEND, W, Q, 1, 1), (SEND, W, Q, 0, 5), (RUN, T_NORM), (SEND, R, X, 0), (SEND, R, X, 2),
    (SEND, R, X, 6), (SEND, W, E, 0, 0), (SEND, W, E, 0, 1), (SEND, W, E, 1, 0), (SEND, W, E, 1, 1),
    (SEND, W, E, 0, 4), (SEND, W, E, 0, 5), (SEND, W, E, 1, 4), (SEND, W, E, 1, 5), (SEND, R, X, 1),
    (SEND, R, X, 3), (WAIT, W, Q, 1, 0), (SEND, W, Q, 1, 6), (SEND, W, Q, 1, 7), (WAIT, W, Q, 0, 0),
    (SEND, W, Q, 0, 6), (SEND, W, Q, 0, 7), (SEND, W, Q, 0, 2), (WAIT, W, Q, 0, 1), (SEND, W, Q, 0, 3),
    (SEND, W, Q, 1, 2), (WAIT, W, Q, 1, 1), (SEND, W, Q, 1, 3), (SEND, W, Q, 0, 8), (SEND, W, Q, 0, 9),
    (SEND, W, Q, 1, 8), (SEND, W, Q, 1, 9), (WAIT, R, X, 0), (SEND, R, X, 4), (WAIT, R, X, 2), (SEND, R, X, 5),
    (WAIT, W, Q, 0, 4), (SEND, W, Q, 0, 12), (WAIT, W, Q, 0, 5), (SEND, W, Q, 0, 13), (WAIT, W, Q, 1, 4),
    (SEND, W, Q, 1, 12), (WAIT, W, Q, 1, 5), (SEND, W, Q, 1, 13), (WAIT, W, Q, 0, 2), (WAIT, W, Q, 0, 3),
    (SEND, W, Q, 0, 10), (SEND, W, Q, 0, 11), (WAIT, W, Q, 1, 2), (WAIT, W, Q, 1, 3), (SEND, W, Q, 1, 10),
    (SEND, W, Q, 1, 11), (WAIT, R, X, 1), (SEND, R, X, 7), (WAIT, R, X, 3), (SEND, R, X, 8), (WAIT, W, Q, 0, 6),
    (SEND, W, Q, 0, 14), (WAIT, W, Q, 0, 7), (SEND, W, Q, 0, 15), (WAIT, W, Q, 1, 6), (SEND, W, Q, 1, 14),
    (WAIT, W, Q, 1, 7), (SEND, W, Q, 1, 15), (WAIT, W, E, 1, 0), (SEND, W, E, 1, 2), (WAIT, W, E, 1, 1),
    (SEND, W, E, 1, 3), (WAIT, W, E, 0, 0), (SEND, W, E, 0, 2), (WAIT, W, E, 0, 1), (SEND, W, E, 0, 3),
    (WAIT, W, Q, 0, 8), (SEND, W, Q, 0, 16), (WAIT, W, Q, 0, 9), (SEND, W, Q, 0, 17), (WAIT, W, Q, 1, 8),
    (SEND, W, Q, 1, 16), (WAIT, W, Q, 1, 9), (SEND, W, Q, 1, 17), (SEND, W, E, 0, 6), (SEND, W, E, 0, 7),
    (SEND, W, E, 1, 6), (SEND, W, E, 1, 7), (WAIT, R, X, 4), (WAIT, R, X, 5), (SEND, R, X, 9), (SEND, R, F, 6),
    (SEND, R, F, 0), (SEND, R, F, 2), (WAIT, W, Q, 0, 10), (SEND, W, Q, 0, 18), (WAIT, W, Q, 0, 11),
    (SEND, W, Q, 0, 19), (WAIT, W, Q, 1, 10), (SEND, W, Q, 1, 18), (WAIT, W, Q, 1, 11), (SEND, W, Q, 1, 19),
    (WAIT, W, E, 0, 4), (SEND, W, E, 0, 12), (WAIT, W, E, 0, 5), (SEND, W, E, 0, 13), (WAIT, W, E, 1, 4),
    (SEND, W, E, 1, 12), (WAIT, W, E, 1, 5), (SEND, W, E, 1, 13), (WAIT, W, Q, 0, 12), (WAIT, W, Q, 0, 13),
    (WAIT, R, X, 6), (WAIT, R, X, 7), (WAIT, R, X, 8), (WAIT, R, X, 9), (RUN, T_PROJECT, Q, 0, 0),
    (WAIT, W, E, 0, 2), (WAIT, W, E, 0, 3), (SEND, W, E, 0, 10), (SEND, W, E, 0, 11), (WAIT, W, E, 1, 2),
    (WAIT, W, E, 1, 3), (SEND, W, E, 1, 10), (SEND, W, E, 1, 11), (WAIT, W, Q, 0, 14), (WAIT, W, Q, 0, 15),
    (RUN, T_PROJECT, Q, 0, 1), (SEND, W, E, 0, 8), (SEND, W, E, 0, 9), (SEND, W, E, 1, 8), (SEND, W, E, 1, 9),
    (WAIT, W, Q, 1, 12), (WAIT, W, Q, 1, 13), (RUN, T_PROJECT, Q, 1, 0), (WAIT, W, Q, 0, 16),
    (WAIT, W, Q, 0, 17), (RUN, T_PROJECT, Q, 0, 2), (SEND, W, C, 0, 0), (SEND, W, C, 0, 1), (SEND, W, C, 1, 0),
    (SEND, W, C, 1, 1), (WAIT, W, Q, 1, 14), (WAIT, W, Q, 1, 15), (RUN, T_PROJECT, Q, 1, 1), (SEND, R, F, 1),
    (SEND, R, F, 3), (WAIT, W, Q, 1, 16), (WAIT, W, Q, 1, 17), (RUN, T_PROJECT, Q, 1, 2), (RUN, T_LOW_RANK),
    (WAIT, W, E, 0, 6), (SEND, W, E, 0, 14), (SEND, W, C, 0, 4), (WAIT, W, E, 0, 7), (SEND, W, E, 0, 15),
    (SEND, W, C, 0, 5), (WAIT, W, E, 1, 6), (SEND, W, E, 1, 14), (SEND, W, C, 1, 4), (WAIT, W, E, 1, 7),
    (SEND, W, E, 1, 15), (SEND, W, C, 1, 5), (RUN, T_RATE, 0, 2), (RUN, T_RATE, 2, 4), (RUN, T_RATE, 4, 6),
    (RUN, T_SUFFIX), (WAIT, W, E, 0, 10), (SEND, W, E, 0, 18), (WAIT, W, E, 0, 11), (SEND, W, E, 0, 19),
    (WAIT, W, E, 1, 10), (SEND, W, E, 1, 18), (WAIT, W, E, 1, 11), (SEND, W, E, 1, 19), (WAIT, W, Q, 0, 18),
    (WAIT, W, Q, 0, 19), (RUN, T_PROJECT, Q, 0, 3), (WAIT, W, E, 0, 8), (SEND, W, E, 0, 16), (WAIT, W, E, 0, 9),
    (SEND, W, E, 0, 17), (WAIT, W, E, 1, 8), (SEND, W, E, 1, 16), (WAIT, W, E, 1, 9), (SEND, W, E, 1, 17),
    (WAIT, W, Q, 1, 18), (WAIT, W, Q, 1, 19), (RUN, T_PROJECT, Q, 1, 3), (WAIT, W, C, 0, 0), (SEND, W, C, 0, 2),
    (WAIT, W, C, 0, 1), (SEND, W, C, 0, 3), (WAIT, W, C, 1, 0), (SEND, W, C, 1, 2), (WAIT, W, C, 1, 1),
    (SEND, W, C, 1, 3), (RUN, T_KEY_STATE), (WAIT, W, E, 0, 12), (WAIT, W, E, 0, 13), (RUN, T_PROJECT, E, 0, 0),
    (SEND, S, 0, 0), (SEND, S, 0, 1), (SEND, W, C, 1, 6), (SEND, W, C, 1, 7), (WAIT, R, F, 0), (SEND, R, F, 4),
    (WAIT, R, F, 2), (SEND, R, F, 5), (WAIT, W, E, 0, 14), (WAIT, W, E, 0, 15), (RUN, T_PROJECT, E, 0, 1),
    (WAIT, W, E, 1, 12), (WAIT, W, E, 1, 13), (RUN, T_PROJECT, E, 1, 0), (WAIT, W, E, 1, 14),
    (WAIT, W, E, 1, 15), (RUN, T_PROJECT, E, 1, 1), (SEND, W, C, 0, 6), (SEND, W, C, 0, 7), (SEND, W, C, 1, 8),
    (SEND, W, C, 1, 9), (WAIT, W, E, 0, 16), (WAIT, W, E, 0, 17), (RUN, T_PROJECT, E, 0, 2),
    (WAIT, W, E, 0, 18), (WAIT, W, E, 0, 19), (RUN, T_PROJECT, E, 0, 3), (WAIT, W, E, 1, 16),
    (WAIT, W, E, 1, 17), (RUN, T_PROJECT, E, 1, 2), (WAIT, W, E, 1, 18), (WAIT, W, E, 1, 19),
    (RUN, T_PROJECT, E, 1, 3), (WAIT, R, F, 1), (SEND, R, F, 7), (WAIT, R, F, 3), (SEND, R, F, 8),
    (RUN, T_LOAD_H), (SEND, W, C, 0, 8), (SEND, W, C, 0, 9), (RUN, T_ATTEND, 0, 3), (RUN, T_ATTEND, 3, 6),
    (WAIT, W, C, 1, 2), (WAIT, W, C, 1, 3), (SEND, W, C, 1, 10), (SEND, W, C, 1, 11), (RUN, T_ATTEND, 6, 9),
    (RUN, T_START_H), (SEND, R, H, 6), (RUN, T_ATTEND, 9, 12), (SEND, R, H, 0), (SEND, R, H, 2),
    (WAIT, S, 0, 0), (SEND, S, 0, 2), (WAIT, S, 0, 1), (SEND, S, 0, 3), (WAIT, W, C, 0, 2), (WAIT, W, C, 0, 3),
    (SEND, W, C, 0, 10), (SEND, W, C, 0, 11), (WAIT, W, C, 1, 4), (SEND, W, C, 1, 12), (WAIT, W, C, 1, 5),
    (SEND, W, C, 1, 13), (WAIT, W, C, 1, 8), (SEND, W, C, 1, 16), (WAIT, W, C, 1, 9), (SEND, W, C, 1, 17),
    (WAIT, R, F, 4), (WAIT, R, F, 5), (SEND, R, F, 9), (WAIT, W, C, 0, 4), (SEND, W, C, 0, 12),
    (WAIT, W, C, 0, 5), (SEND, W, C, 0, 13), (WAIT, W, C, 1, 6), (SEND, W, C, 1, 14), (WAIT, W, C, 1, 7),
    (SEND, W, C, 1, 15), (WAIT, S, 0, 2), (WAIT, S, 0, 3), (RUN, T_FOLD_Y), (WAIT, W, C, 0, 8),
    (SEND, W, C, 0, 16), (WAIT, W, C, 0, 9), (SEND, W, C, 0, 17), (SEND, S, 1, 0), (SEND, S, 1, 1),
    (WAIT, W, C, 0, 6), (SEND, W, C, 0, 14), (WAIT, W, C, 0, 7), (SEND, W, C, 0, 15), (WAIT, W, C, 1, 12),
    (WAIT, W, C, 1, 13), (RUN, T_PROJECT, C, 1, 0), (WAIT, W, C, 1, 10), (SEND, W, C, 1, 18),
    (WAIT, W, C, 1, 11), (SEND, W, C, 1, 19), (SEND, R, H, 1), (SEND, R, H, 3), (WAIT, W, C, 0, 10),
    (SEND, W, C, 0, 18), (WAIT, W, C, 0, 11), (SEND, W, C, 0, 19), (SEND, W, D, 0, 0), (SEND, W, D, 0, 1),
    (SEND, W, D, 1, 0), (SEND, W, D, 1, 1), (WAIT, W, C, 1, 14), (WAIT, W, C, 1, 15), (RUN, T_PROJECT, C, 1, 1),
    (WAIT, W, C, 0, 12), (WAIT, W, C, 0, 13), (RUN, T_PROJECT, C, 0, 0), (WAIT, W, C, 1, 16),
    (WAIT, W, C, 1, 17), (RUN, T_PROJECT, C, 1, 2), (WAIT, S, 1, 0), (SEND, S, 1, 2), (WAIT, S, 1, 1),
    (SEND, S, 1, 3), (SEND, W, D, 0, 4), (SEND, W, D, 0, 5), (SEND, W, D, 1, 4), (SEND, W, D, 1, 5),
    (WAIT, W, C, 0, 14), (WAIT, W, C, 0, 15), (RUN, T_PROJECT, C, 0, 1), (WAIT, W, C, 0, 16),
    (WAIT, W, C, 0, 17), (RUN, T_PROJECT, C, 0, 2), (WAIT, W, C, 1, 18), (WAIT, W, C, 1, 19),
    (RUN, T_PROJECT, C, 1, 3), (WAIT, W, C, 0, 18), (WAIT, W, C, 0, 19), (RUN, T_PROJECT, C, 0, 3),
    (RUN, T_GATE, C), (WAIT, R, H, 0), (SEND, R, H, 4), (WAIT, R, H, 2), (SEND, R, H, 5), (RUN, T_CONV, C),
    (WAIT, W, D, 0, 0), (SEND, W, D, 0, 2), (WAIT, W, D, 0, 1), (SEND, W, D, 0, 3), (SEND, W, D, 0, 6),
    (SEND, W, D, 0, 7), (WAIT, W, D, 1, 0), (SEND, W, D, 1, 6), (SEND, W, D, 1, 7), (WAIT, S, 1, 2),
    (WAIT, S, 1, 3), (RUN, T_FOLD_Z), (RUN, T_FIRST_ROWS, C), (RUN, T_PAIR_PRODUCTS, 0),
    (RUN, T_PAIR_PRODUCTS, 1), (SEND, W, D, 1, 2), (WAIT, W, D, 1, 1), (SEND, W, D, 1, 3),
    (RUN, T_PAIR_PRODUCTS, 2), (RUN, T_PAIR_PRODUCTS, 3), (WAIT, R, H, 1), (SEND, R, H, 7), (WAIT, R, H, 3),
    (SEND, R, H, 8), (RUN, T_FAR, 0), (RUN, T_FAR, 1), (WAIT, W, D, 0, 4), (SEND, W, D, 0, 12),
    (WAIT, W, D, 0, 5), (SEND, W, D, 0, 13), (WAIT, W, D, 1, 4), (SEND, W, D, 1, 12), (WAIT, W, D, 1, 5),
    (SEND, W, D, 1, 13), (RUN, T_FAR, 2), (RUN, T_FAR, 3), (WAIT, W, D, 0, 2), (WAIT, W, D, 0, 3),
    (SEND, W, D, 0, 10), (SEND, W, D, 0, 11), (SEND, W, D, 1, 8), (SEND, W, D, 1, 9), (WAIT, W, D, 0, 6),
    (SEND, W, D, 0, 14), (WAIT, W, D, 0, 7), (SEND, W, D, 0, 15), (WAIT, W, D, 1, 2), (WAIT, W, D, 1, 3),
    (SEND, W, D, 1, 10), (SEND, W, D, 1, 11), (SEND, W, D, 0, 8), (SEND, W, D, 0, 9), (WAIT, W, D, 0, 12),
    (WAIT, W, D, 0, 13), (RUN, T_PROJECT, D, 0, 0), (WAIT, W, D, 1, 12), (WAIT, W, D, 1, 13),
    (RUN, T_PROJECT, D, 1, 0), (WAIT, R, H, 4), (WAIT, R, H, 5), (SEND, R, H, 9), (WAIT, W, D, 1, 6),
    (SEND, W, D, 1, 14), (WAIT, W, D, 1, 7), (SEND, W, D, 1, 15), (RUN, T_NEAR, 0), (WAIT, W, D, 0, 10),
    (SEND, W, D, 0, 18), (WAIT, W, D, 0, 11), (SEND, W, D, 0, 19), (WAIT, W, D, 1, 8), (SEND, W, D, 1, 16),
    (WAIT, W, D, 1, 9), (SEND, W, D, 1, 17), (RUN, T_NEAR, 1), (RUN, T_NEAR, 2), (WAIT, W, D, 0, 14),
    (WAIT, W, D, 0, 15), (RUN, T_PROJECT, D, 0, 1), (RUN, T_NEAR, 3), (WAIT, W, D, 1, 10), (SEND, W, D, 1, 18),
    (WAIT, W, D, 1, 11), (SEND, W, D, 1, 19), (RUN, T_GATHER, 0), (RUN, T_PAIR_PRODUCTS, 4), (WAIT, W, D, 0, 8),
    (SEND, W, D, 0, 16), (WAIT, W, D, 0, 9), (SEND, W, D, 0, 17), (WAIT, W, D, 1, 14), (WAIT, W, D, 1, 15),
    (RUN, T_PROJECT, D, 1, 1), (RUN, T_GATHER, 1), (RUN, T_PAIR_PRODUCTS, 5), (RUN, T_FAR, 4),
    (WAIT, W, D, 1, 16), (WAIT, W, D, 1, 17), (RUN, T_PROJECT, D, 1, 2), (RUN, T_GATHER, 2),
    (RUN, T_PAIR_PRODUCTS, 6), (RUN, T_FAR, 5), (WAIT, W, D, 1, 18), (WAIT, W, D, 1, 19),
    (RUN, T_PROJECT, D, 1, 3), (RUN, T_GATHER, 3), (RUN, T_PAIR_PRODUCTS, 7), (RUN, T_NEAR, 4),
    (WAIT, W, D, 0, 16), (WAIT, W, D, 0, 17), (RUN, T_PROJECT, D, 0, 2), (WAIT, W, D, 0, 18),
    (WAIT, W, D, 0, 19), (RUN, T_PROJECT, D, 0, 3), (RUN, T_NEAR, 5), (RUN, T_GATE, D), (RUN, T_CONV, D),
    (RUN, T_FAR, 6), (RUN, T_FAR, 7), (RUN, T_GATHER, 4), (RUN, T_FIRST_ROWS, D), (RUN, T_EXCHANGE),
    (RUN, T_GATHER, 5), (RUN, T_NEAR, 6), (RUN, T_NEAR, 7), (WAIT, R, F, 6), (WAIT, R, F, 7), (WAIT, R, F, 8),
    (WAIT, R, F, 9), (WAIT, R, H, 6), (WAIT, R, H, 7), (WAIT, R, H, 8), (WAIT, R, H, 9), (RUN, T_COLLECT),
    (RUN, T_LAST, 0), (RUN, T_LAST, 1), (RUN, T_LAST, 2), (RUN, T_LAST, 3), (RUN, T_LAST, 4),
    (RUN, T_GATHER, 6), (RUN, T_LAST, 5), (RUN, T_LAST, 6), (RUN, T_GATHER, 7), (RUN, T_LAST, 7),
)


def layer_kernel(
    x_in,
    gain,
    w_q,
    w_k,
    w_v,
    w_out,
    w_in,
    w_src,
    left,
    right,
    offset,
    spikes,
    head_gain,
    taps,
    w_a,
    w_c,
    out,
    xs,
    qab,
    ca,
    cb,
    da,
    db,
    wf,
    wo,
    acc_a,
    acc_b,
    krows,
    vrows,
    low,
    within,
    tail,
    spk,
    inside,
    q_far,
    state,
    prefix,
    st_send,
    dec_send,
    st_recv,
    dec_recv,
    gated_c,
    gated_d,
    mix,
    late_mix,
    late_recv,
    own,
    sib_send,
    sib_recv,
    far_send,
    far_recv,
    near_send,
    near_recv,
    load_sem,
    out_sem,
    w_send,
    w_recv,
    x_send,
    x_recv,
    s_send,
    s_recv,
    h_send,
    h_recv,
    e_send,
    e_recv,
    ss,
    sr,
    fs,
    fr,
    ns,
    nr,
    free_sem,
):
    z = lax.axis_index("sp_0")
    y = lax.axis_index("sp_1")
    t = lax.axis_index("tp")
    core = t % 2
    xi = t // 2
    sp = z * 4 + y
    sp_next = (sp + 1) % 16
    sp_prev = (sp + 15) % 16
    to_next = {"sp_0": sp_next // 4, "sp_1": sp_next % 4}
    to_prev = {"sp_0": sp_prev // 4, "sp_1": sp_prev % 4}
    to_sib = {"tp": xi * 2 + (1 - core)}

    def at_z(d):
        return {"sp_0": (z + d) % 4}

    def at_y(d):
        return {"sp_1": (y + d) % 4}

    def at_x(d):
        return {"tp": ((xi + d) % 4) * 2 + core}

    def remote(ref, dst, sems, at, to):
        return pltpu.make_async_remote_copy(
            src_ref=ref,
            dst_ref=dst,
            send_sem=sems[0].at[at],
            recv_sem=sems[1].at[at],
            device_id=to,
            device_id_type=MESH,
        )

    own0 = pl.ds(pl.multiple_of(sp * KB, KB), KB)
    own1 = pl.ds(pl.multiple_of((y * 4 + z) * KB, KB), KB)
    own1_v = pl.ds(pl.multiple_of(MODEL + (y * 4 + z) * KB, KB), KB)
    own_rows = pl.multiple_of(t * ROWS, 32)
    loads = [
        (x_in, xs.at[pl.ds(own_rows, ROWS), :]),
        (w_k, qab.at[own0, 0:256]),
        (w_v.at[:, 0:128], qab.at[own0, 256:384]),
        (w_q.at[:, 0:128], qab.at[own0, 384:512]),
        (w_v.at[:, 128:512], qab.at[own1_v, 0:384]),
        (w_q.at[:, 128:256], qab.at[own1_v, 384:512]),
        (w_in.at[:, 128:256], ca.at[own0, 0:128]),
        (w_src.at[:, 0:256], ca.at[own0, 128:384]),
        (w_out.at[:, 0:256], cb.at[own1, 0:256]),
        (w_in.at[:, 0:128], cb.at[own1, 256:384]),
        (w_in.at[:, 384:512], da.at[own0, 0:128]),
        (w_src.at[:, 256:512], da.at[own0, 128:384]),
        (w_out.at[:, 256:512], db.at[own1, 0:256]),
        (w_in.at[:, 256:384], db.at[own1, 256:384]),
        (w_c.at[EARLY : EARLY + 128, :], wf.at[pl.ds(pl.multiple_of(t * 128, 128), 128), :]),
    ]
    loads = [pltpu.make_async_copy(a, b, load_sem.at[i]) for i, (a, b) in enumerate(loads)]
    for c in loads:
        c.start()

    barrier = pltpu.get_barrier_semaphore()
    peers = [at_z(1), at_z(3), at_y(1), at_y(3), to_next, to_prev] + [{"tp": (t + d) % 8} for d in range(1, 8)]
    for p in peers:
        pl.semaphore_signal(barrier, inc=1, device_id=p, device_id_type=MESH)

    def h_loads():
        return [
            pltpu.make_async_copy(
                w_c.at[EARLY + 128 : 512, pl.ds(i * 512, 512)],
                qab.at[pl.ds(pl.multiple_of(t * 1024 + i * 128, 128), 128), :],
                load_sem.at[14 + i],
            )
            for i in range(8)
        ]

    def out_loads(i):
        cols = pl.ds(i * CW, CW)
        return (
            pltpu.make_async_copy(w_a.at[:, cols], wo.at[i % 3, 0:512, :], out_sem.at[2 * i]),
            pltpu.make_async_copy(w_c.at[0:EARLY, cols], wo.at[i % 3, 512:MIX, :], out_sem.at[2 * i + 1]),
        )

    for c in loads[1:]:
        c.wait()
    pl.semaphore_wait(barrier, len(peers))

    started = []
    started_q = []

    def go(c, group=None):
        c.start()
        (started_q if group in ("q", "e") else started).append(c)

    bufs = {"q": (qab, qab), "e": (qab, qab), "c": (ca, cb), "d": (da, db)}
    first_row = {"q": (0, MODEL), "e": (0, MODEL), "c": (0, 0), "d": (0, 0)}
    lanes = {"q": slice(0, 384), "e": slice(384, 512), "c": slice(0, 384), "d": slice(0, 384)}
    base = {"q": 0, "c": 2, "d": 4, "e": 6}
    rings = {"x": (xs, ROWS, 0), "f": (wf, 128, 10), "h": (qab, 1024, 20)}
    xm, xp, xf = (xi + 3) % 4, (xi + 1) % 4, (xi + 2) % 4

    def w_copy(g, path, slot, du, dv, axis, step, row=0, rows=KB):
        u0, v0 = (z, y) if path == 0 else (y, z)
        j = ((u0 + du) % 4) * 4 + (v0 + dv) % 4
        ref = bufs[g][path].at[pl.ds(pl.multiple_of(first_row[g][path] + j * KB + row, 128), rows), lanes[g]]
        to = at_z(step) if (axis == 0) == (path == 0) else at_y(step)
        return remote(ref, ref, (w_send, w_recv), (base[g] + path, slot), to)

    def ring_copy(n, slot, x_from, top, halves, to, c=None):
        buf, rows, first = rings[n]
        half = rows // 2
        at = (x_from * 2 + (core if c is None else c)) * rows + (0 if top else half)
        ref = buf.at[pl.ds(pl.multiple_of(at, 16), half * halves), :]
        return remote(ref, ref, (x_send, x_recv), first + slot, to)

    right_x, left_x = at_x(1), at_x(3)

    def st_copy(ph, slot):
        to = (at_y if ph == 0 else at_z)(1 if slot % 2 == 0 else 3)
        i = ph * 3
        if slot < 2:
            a, b = st_send.at[ph], st_recv.at[i + 2 * slot]
        else:
            half = pl.ds((slot - 2) * VAL, VAL)
            a, b = st_recv.at[i + 2 * (slot - 2), half, :], st_recv.at[i + 1, half, :]
        return remote(a, b, (s_send, s_recv), ph * 8 + slot, to)

    def dec_copy(ph, slot):
        to = (at_y if ph == 0 else at_z)(1 if slot != 1 else 3)
        i = ph * 3
        if slot < 2:
            a, b = dec_send.at[ph], dec_recv.at[i + 2 * slot]
        else:
            a, b = dec_recv.at[i], dec_recv.at[i + 1]
        return remote(a, b, (s_send, s_recv), ph * 8 + 4 + slot, to)

    def halo_copy(g):
        buf = gated_c if g == "c" else gated_d
        i = 0 if g == "c" else 1
        return remote(buf.at[pl.ds(TOK, 8), :], buf.at[pl.ds(0, 8), :], (h_send, h_recv), i, to_next)

    def sib_copy(c):
        return remote(sib_send.at[c % 2], sib_recv.at[c], (ss, sr), c, to_sib)

    def far_copy(c, side):
        return remote(far_send.at[c % 4, side], far_recv.at[c, side], (fs, fr), (c, side), right_x if side == 0 else left_x)

    def near_copy(c, side):
        return remote(near_send.at[c % 4, side], near_recv.at[c, side], (ns, nr), (c, side), right_x if side == 0 else left_x)

    def late_copy(d, sending):
        g = (t + d) % 8
        me = t if sending else (t + 8 - d) % 8
        src = late_mix.at[pl.ds(pl.multiple_of(g * ROWS, 32), ROWS), :]
        return remote(src, late_recv.at[me], (e_send, e_recv), d - 1, {"tp": g})

    def w_sent(g, p, slot):
        if slot < 2:
            return w_copy(g, p, slot, 0, 0, 0, 1 + 2 * slot)
        if slot < 4:
            return w_copy(g, p, slot, 3 if slot == 2 else 1, 0, 0, 1 if slot == 2 else 3, 128 * (slot - 2), 128)
        k, side = DELTA[(slot - 4) % 8 // 2], slot % 2
        if slot < 12:
            return w_copy(g, p, slot, k, 0, 1, 1 + 2 * side)
        return w_copy(g, p, slot, k, 1 if side else 3, 1, 1 + 2 * side, 128 * side, 128)

    def w_came(g, p, slot):
        side = slot % 2
        step, row = 1 + 2 * side, 128 * side
        if slot < 2:
            return w_copy(g, p, slot, 1 if side else 3, 0, 0, step)
        if slot < 4:
            return w_copy(g, p, slot, 2, 0, 0, step, row, 128)
        k = DELTA[(slot - 4) % 8 // 2]
        if slot < 12:
            return w_copy(g, p, slot, k, 1 if side else 3, 1, step)
        return w_copy(g, p, slot, k, 2, 1, step, row, 128)

    ring_sent = (
        (0, True, 1, 1), (0, False, 1, 1), (0, False, 1, 3), (0, True, 1, 3), (3, True, 1, 1), (1, False, 1, 3),
        (0, True, 2, 0), (3, True, 2, 0), (1, True, 2, 0), (2, True, 2, 0),
    )
    ring_came = (
        (3, True, 1, 1), (3, False, 1, 1), (1, False, 1, 3), (1, True, 1, 3), (2, True, 1, 1), (2, False, 1, 3),
        (0, True, 2, 0), (3, True, 2, 0), (1, True, 2, 0), (2, True, 2, 0),
    )

    def ring(n, slot, came):
        d, top, halves, step = (ring_came if came else ring_sent)[slot]
        to = to_sib if step == 0 else at_x(step)
        other = came and step == 0
        return ring_copy(n, slot, (xi + d) % 4, top, halves, to, 1 - core if other else None)

    def head(h):
        return slice(h * KEY, (h + 1) * KEY), slice(h * VAL, (h + 1) * VAL)

    class Device:
        def send(self, kind, *a):
            if kind == "w":
                go(w_sent(*a), a[0])
            elif kind == "r":
                go(ring(*a, False))
            else:
                go(st_copy(*a))
                if a[1] < 3:
                    go(dec_copy(*a))

        def wait(self, kind, *a):
            if kind == "w":
                w_came(*a).wait_recv()
            elif kind == "r":
                ring(*a, True).wait_recv()
            elif kind == "s":
                st_copy(*a).wait_recv()
                if a[1] < 3:
                    dec_copy(*a).wait_recv()

        def norm(self):
            loads[0].wait()

            def step(i, _):
                r = pl.ds(pl.multiple_of(own_rows + i * 16, 16), 16)
                v = xs[r, :].astype(F32)
                inv = lax.rsqrt(jnp.mean(v * v, axis=-1, keepdims=True) + EPS)
                g = gain[...].astype(F32)
                for c in range(32):
                    k = slice(c * 128, (c + 1) * 128)
                    xs[r, k] = (v[:, k] * inv * g[c : c + 1, :]).astype(BF16)
                return 0

            lax.fori_loop(0, ROWS // 16, step, 0)
            spk[...] = jnp.zeros_like(spk)
            spk[0:2, :] = spikes[...]
            for i in range(3):
                for c in out_loads(i):
                    c.start()

        def low_rank(self):
            low[...] = nt(xs[...], left[...]).astype(BF16)

        def rate(self, lo, hi):
            lane_head = lax.broadcasted_iota(jnp.int32, (8, 2 * KEY), 1) // KEY
            pick = jnp.where(lax.broadcasted_iota(jnp.int32, (8, 2 * KEY), 0) == lane_head, 1.0, 0.0).astype(F32)
            row = lax.broadcasted_iota(jnp.int32, (128, 128), 0)
            col = lax.broadcasted_iota(jnp.int32, (128, 128), 1)
            low_tri = jnp.where((row >= col) & (row // BLOCK == col // BLOCK), 1.0, 0.0).astype(F32)

            def step(i, _):
                r = pl.ds(pl.multiple_of(i * 128, 128), 128)
                g = mm(low[r, :], right[...]) + offset[...]
                ls = jnp.minimum(g, 0.0) - jnp.log1p(jnp.exp(-jnp.abs(g)))
                spike = lax.dot_general(
                    spk[:, r], pick, (((0,), (0,)), ((), ())), precision=HIGHEST, preferred_element_type=F32
                )
                within[r, :] = jnp.dot(
                    low_tri, ls * (1.0 / 16.0) + spike, precision=HIGHEST, preferred_element_type=F32
                )
                return 0

            lax.fori_loop(lo, hi, step, 0)

        def suffix(self):
            prefix[0:1, :] = jnp.zeros((1, 2 * KEY), F32)

            def back(i, _):
                n = TOK // BLOCK - 1 - i
                w = within[pl.ds(pl.multiple_of(n * BLOCK, BLOCK), BLOCK), :]
                end = w[BLOCK - 1 : BLOCK, :]
                later = prefix[0:1, :]
                tail[pl.ds(pl.multiple_of(n * BLOCK, BLOCK), BLOCK), :] = jnp.exp(end - w + later).astype(BF16)
                prefix[0:1, :] = later + end
                return 0

            lax.fori_loop(0, TOK // BLOCK, back, 0)
            dec_send[0] = jnp.broadcast_to(jnp.exp(prefix[0:1, :]), (8, 2 * KEY))

        def project(self, g, p, k):
            w, acc = bufs[g][p], (acc_a, acc_b)[p]
            u = ((z if p == 0 else y) + DELTA[k]) % 4
            if p == 0:
                lhs = xs[:, pl.ds(pl.multiple_of(u * 1024, 1024), 1024)]
            else:
                lhs = jnp.concatenate(
                    [xs[:, pl.ds(pl.multiple_of((v * 4 + u) * KB, KB), KB)] for v in range(4)], axis=1
                )
            cols = lanes[g]
            part = mm(lhs, w[pl.ds(pl.multiple_of(first_row[g][p] + u * 1024, 1024), 1024), cols])
            if k == 0:
                acc[:, cols] = part
            else:
                acc[:, cols] += part

        def key_state(self):
            def step(i, _):
                r = pl.ds(pl.multiple_of(i * 64, 64), 64)
                krows[r, :] = acc_a[r, 0:256].astype(BF16)
                vrows[r, 0:128] = acc_a[r, 256:384].astype(BF16)
                vrows[r, 128:512] = acc_b[r, 0:384].astype(BF16)
                return 0

            lax.fori_loop(0, TOK // 64, step, 0)
            k_tail = (krows[...].astype(F32) * tail[...].astype(F32)).astype(BF16)
            for h in range(2):
                kc, vc = head(h)
                s = tn(vrows[:, vc], k_tail[:, kc])
                st_send[0, vc, :] = s.astype(BF16)
            state[...] = jnp.zeros_like(state)
            prefix[0:1, :] = jnp.zeros((1, 2 * KEY), F32)

        def attend(self, lo, hi):
            def step(n, _):
                r = pl.ds(pl.multiple_of(n * BLOCK, BLOCK), BLOCK)
                row = lax.broadcasted_iota(jnp.int32, (BLOCK, BLOCK), 0)
                col = lax.broadcasted_iota(jnp.int32, (BLOCK, BLOCK), 1)
                causal = row >= col
                w = within[r, :]
                end = w[BLOCK - 1 : BLOCK, :]
                mid = end * 0.5
                q_now = jnp.concatenate([acc_a[r, 384:512], acc_b[r, 384:512]], axis=1).astype(BF16)
                q_s = q_now.astype(F32) * (KEY**-0.5) * jnp.exp(w - mid)
                k_s = krows[r, :].astype(F32) * jnp.exp(mid - w)
                e_mid = jnp.exp(mid)
                q_d = q_s * e_mid
                k_t = (k_s * e_mid).astype(BF16)
                e_end = jnp.exp(end)
                before = prefix[0:1, :]
                q_far[r, :] = (q_d * jnp.exp(before)).astype(BF16)
                prefix[0:1, :] = before + end
                q_d = q_d.astype(BF16)
                q_s = q_s.astype(BF16)
                k_s = k_s.astype(BF16)
                for h in range(2):
                    kc, vc = head(h)
                    v = vrows[r, vc]
                    scores = jnp.where(causal, nt(q_s[:, kc], k_s[:, kc]), 0.0).astype(BF16)
                    s = state[vc, :]
                    inside[r, vc] = mm(scores, v) + nt(q_d[:, kc], s.astype(BF16))
                    state[vc, :] = s * e_end[:, kc] + tn(v, k_t[:, kc])
                return 0

            lax.fori_loop(lo, hi, step, 0)

        def fold(self, total, decay, i, use):
            dec = jnp.where(use, dec_recv[i][0:1, :], 1.0)
            out_ = []
            for h in range(2):
                kc, vc = head(h)
                got = jnp.where(use, st_recv[i, vc, :].astype(F32), 0.0)
                out_.append(total[h] * dec[:, kc] + got)
            return out_, decay * dec

        def fold_y(self):
            own_decay = dec_send[0][0:1, :]
            total = [jnp.zeros((VAL, KEY), F32) for _ in range(2)]
            decay = jnp.ones((1, 2 * KEY), F32)
            for d in (3, 2, 1):
                total, decay = self.fold(total, decay, d - 1, d <= y)
            prefix[1:2, :] = decay
            for h in range(2):
                kc, vc = head(h)
                state[vc, :] = total[h]
                total[h] = total[h] * own_decay[:, kc] + st_send[0, vc, :].astype(F32)
            decay = decay * own_decay
            for d in (3, 2, 1):
                total, decay = self.fold(total, decay, d - 1, d > y)
            for h in range(2):
                kc, vc = head(h)
                st_send[1, vc, :] = total[h].astype(BF16)
            dec_send[1] = jnp.broadcast_to(decay, (8, 2 * KEY))

        def fold_z(self):
            total = [jnp.zeros((VAL, KEY), F32) for _ in range(2)]
            decay = jnp.ones((1, 2 * KEY), F32)
            for d in (3, 2, 1):
                total, decay = self.fold(total, decay, 3 + d - 1, d <= z)
            decay = prefix[1:2, :]
            for h in range(2):
                kc, vc = head(h)
                state[vc, :] = total[h] * decay[:, kc] + state[vc, :]
            hg = head_gain[...].astype(F32)

            def finish(g, _):
                r = pl.ds(pl.multiple_of(g * ROWS, 32), ROWS)
                to = self.place(g)
                for h in range(2):
                    kc, vc = head(h)
                    a = inside[r, vc] + nt(q_far[r, kc], state[vc, :].astype(BF16))
                    ms = jnp.mean(a * a, axis=-1, keepdims=True)
                    mix[to, vc] = (a * lax.rsqrt(ms + EPS) * hg[h : h + 1, :]).astype(BF16)
                return 0

            lax.fori_loop(0, 8, finish, 0)

        def place(self, g):
            mine = 1 - (g + core) % 2
            d = (g // 2 + 4 - xi) % 4
            return pl.ds(pl.multiple_of((mine * 4 + d) * ROWS, 32), ROWS)

        def gate(self, g):
            gated = gated_c if g == "c" else gated_d

            def rnd(v):
                return v.astype(BF16).astype(F32)

            def step(i, _):
                r = pl.ds(pl.multiple_of(i * 64, 64), 64)
                o = pl.ds(pl.multiple_of(i * 64 + 8, 8), 64)
                gated[o, 0:128] = rnd(rnd(acc_b[r, 256:384]) * rnd(acc_a[r, 128:256]))
                gated[o, 128:256] = rnd(rnd(acc_a[r, 0:128]) * rnd(acc_a[r, 256:384]))
                return 0

            lax.fori_loop(0, TOK // 64, step, 0)
            go(halo_copy(g))

        def rows(self, g, i):
            gated = gated_c if g == "c" else gated_d
            tp = taps[...].astype(F32)[:, slice(0, EARLY) if g == "c" else slice(EARLY, 512)]
            block = gated[pl.ds(pl.multiple_of(i * ROWS, 32), ROWS + 8), :]
            if isinstance(i, int):
                keep = jnp.where(sp == 0, 0.0, 1.0)
                rim = lax.broadcasted_iota(jnp.int32, (ROWS + 8, 1), 0) < 8
                block = jnp.where(rim, block * keep, block)
            one = pltpu.roll(block, 1, 0)[8:, :]
            two = pltpu.roll(block, 2, 0)[8:, :]
            s = tp[0:1, :] * two + tp[1:2, :] * one + tp[2:3, :] * block[8:, :]
            r = pl.ds(pl.multiple_of(i * ROWS, 32), ROWS)
            s = (s * acc_b[r, 0:256].astype(BF16).astype(F32)).astype(BF16)
            if g == "c":
                mix[self.place(i), 512:MIX] = s
            else:
                late_mix[r, :] = s

        def conv(self, g):
            def step(i, _):
                self.rows(g, i)
                return 0

            lax.fori_loop(1, 8, step, 0)

        def first_rows(self, g):
            halo_copy(g).wait_recv()
            self.rows(g, 0)

        def load_h(self):
            for c in started_q:
                c.wait_send()
            for c in h_loads():
                c.start()
            for to in (at_x(1), at_x(3), to_sib):
                pl.semaphore_signal(free_sem, inc=1, device_id=to, device_id_type=MESH)

        def start_h(self):
            for c in h_loads():
                c.wait()
            pl.semaphore_wait(free_sem, 3)

        def pair_products(self, i):
            for c in out_loads(i):
                c.wait()
            if i >= 2:
                sib_copy(i - 2).wait_send()
            sib_send[i % 2] = mm(mix[0 : 4 * ROWS, :], wo[i % 3]).astype(BF16)
            sib_copy(i).start()
            own[i % 4] = mm(mix[4 * ROWS : TOK, :], wo[i % 3])
            if i + 3 < CHUNKS:
                for c in out_loads(i + 3):
                    c.start()

        def pair(self, c, d, r0, rows):
            at = slice(d * ROWS + r0, d * ROWS + r0 + rows)
            return own[c % 4, at, :] + sib_recv[c, at, :].astype(F32)

        def far(self, c):
            sib_copy(c).wait_recv()
            for side in (0, 1):
                if c >= 4:
                    far_copy(c - 4, side).wait_send()
                far_send[c % 4, side] = self.pair(c, 2, side * 48, 48).astype(BF16)
                far_copy(c, side).start()

        def near(self, c):
            for side in (0, 1):
                d = 1 + 2 * side
                if c >= 4:
                    near_copy(c - 4, side).wait_send()
                far_copy(c, side).wait_recv()
                for half in (0, 1):
                    v = self.pair(c, d, 48 * half, 48)
                    if half == side:
                        v = v + far_recv[c, side].astype(F32)
                    near_send[c % 4, side, 48 * half : 48 * half + 48, :] = v.astype(BF16)
                near_copy(c, side).start()

        def gather(self, c):
            near_copy(c, 0).wait_recv()
            near_copy(c, 1).wait_recv()
            total = self.pair(c, 0, 0, ROWS) + near_recv[c, 0].astype(F32) + near_recv[c, 1].astype(F32)
            inside[c * ROWS : (c + 1) * ROWS, :] = total

        def exchange(self):
            for d in (1, 7, 2, 6, 3, 5, 4):
                go(late_copy(d, True))
            late_recv[t] = late_mix[pl.ds(own_rows, ROWS), :]

        def collect(self):
            for d in range(1, 8):
                late_copy(d, False).wait_recv()

        def last(self, i):
            k = slice(i * CW, (i + 1) * CW)
            lhs_f = jnp.concatenate([late_recv[g, :, 0:128] for g in range(8)], axis=1)
            lhs_h = jnp.concatenate([late_recv[g, :, 128:256] for g in range(8)], axis=1)
            w_h = jnp.concatenate([qab[g * 1024 + i * 128 : g * 1024 + (i + 1) * 128, :] for g in range(8)], axis=0)
            total = inside[i * ROWS : (i + 1) * ROWS, :] + mm(lhs_f, wf[:, k]) + mm(lhs_h, w_h)
            out[:, k] = total.astype(BF16)

        def close(self):
            for i in range(CHUNKS - 2, CHUNKS):
                sib_copy(i).wait_send()
            for i in range(CHUNKS - 4, CHUNKS):
                for side in (0, 1):
                    far_copy(i, side).wait_send()
                    near_copy(i, side).wait_send()
            for c in started:
                c.wait_send()

    device = Device()
    for kind, *what in ORDER:
        if kind == "run":
            getattr(device, what[0])(*what[1:])
        else:
            getattr(device, kind)(*what)
    device.close()


def layer(*args):
    any_ = pl.BlockSpec(memory_space=pl.ANY)
    vmem = pl.BlockSpec(memory_space=pltpu.VMEM)
    dma = pltpu.SemaphoreType.DMA

    def f32(*shape):
        return pltpu.VMEM(shape, F32)

    def bf16(*shape):
        return pltpu.VMEM(shape, BF16)

    return pl.pallas_call(
        layer_kernel,
        out_shape=jax.ShapeDtypeStruct((ROWS, MODEL), BF16),
        in_specs=[any_, vmem] + [any_] * 6 + [vmem] * 6 + [any_] * 2,
        out_specs=vmem,
        scratch_shapes=[
            bf16(TOK, MODEL),
            bf16(2 * MODEL, 512),
            bf16(MODEL, 384),
            bf16(MODEL, 384),
            bf16(MODEL, 384),
            bf16(MODEL, 384),
            bf16(8 * 128, MODEL),
            bf16(3, MIX, CW),
            f32(TOK, 512),
            f32(TOK, 512),
            bf16(TOK, 2 * KEY),
            bf16(TOK, 2 * VAL),
            bf16(TOK, 64),
            f32(TOK, 2 * KEY),
            bf16(TOK, 2 * KEY),
            f32(8, TOK),
            f32(TOK, 2 * VAL),
            bf16(TOK, 2 * KEY),
            f32(2 * VAL, KEY),
            f32(8, 2 * KEY),
            bf16(2, 2 * VAL, KEY),
            f32(2, 8, 2 * KEY),
            bf16(6, 2 * VAL, KEY),
            f32(6, 8, 2 * KEY),
            f32(TOK + 8, EARLY),
            f32(TOK + 8, LATE),
            bf16(TOK, MIX),
            bf16(TOK, LATE),
            bf16(8, ROWS, LATE),
            f32(4, 4 * ROWS, CW),
            bf16(2, 4 * ROWS, CW),
            bf16(CHUNKS, 4 * ROWS, CW),
            bf16(4, 2, 48, CW),
            bf16(CHUNKS, 2, 48, CW),
            bf16(4, 2, ROWS, CW),
            bf16(CHUNKS, 2, ROWS, CW),
            dma((22,)),
            dma((2 * CHUNKS,)),
            dma((8, 20)),
            dma((8, 20)),
            dma((30,)),
            dma((30,)),
            dma((16,)),
            dma((16,)),
            dma((2,)),
            dma((2,)),
            dma((7,)),
            dma((7,)),
            dma((CHUNKS,)),
            dma((CHUNKS,)),
            dma((CHUNKS, 2)),
            dma((CHUNKS, 2)),
            dma((CHUNKS, 2)),
            dma((CHUNKS, 2)),
            pltpu.SemaphoreType.REGULAR,
        ],
        compiler_params=pltpu.CompilerParams(
            collective_id=0, has_side_effects=True, vmem_limit_bytes=67_000_000
        ),
        name="layer",
    )(*args)


def body(
    hidden_activations,
    entry_rescale_vector,
    probe_matrix,
    lookup_address_matrix,
    payload_matrix,
    postfilter_switch_matrix,
    prefilter_switch_matrix,
    filter_source_matrix,
    forget_left_factor,
    forget_right_factor,
    forget_offset_per_feature,
    forget_spike_additions,
    subspace_rescale_vector,
    depthwise_filter_taps,
    mixer_result_matrix,
    filter_result_matrix,
):
    return layer(
        hidden_activations,
        entry_rescale_vector.reshape(32, 128),
        probe_matrix,
        lookup_address_matrix,
        payload_matrix,
        postfilter_switch_matrix,
        prefilter_switch_matrix,
        filter_source_matrix,
        forget_left_factor.T,
        forget_right_factor,
        forget_offset_per_feature[None, :],
        forget_spike_additions,
        subspace_rescale_vector,
        depthwise_filter_taps,
        mixer_result_matrix,
        filter_result_matrix,
    )


def solution(mesh):
    split = Mesh(mesh.devices.reshape(4, 4, mesh.shape["tp"]), ("sp_0", "sp_1", "tp"))
    in_specs = (
        P(SP_TP, None),
        P(),
        P(SP, "tp"),
        P(SP, "tp"),
        P(SP, "tp"),
        P(SP, "tp"),
        P(SP, "tp"),
        P(SP, "tp"),
        P(),
        P(None, "tp"),
        P("tp"),
        P("tp", SP),
        P("tp", None),
        P(None, "tp"),
        P("tp", None),
        P("tp", None),
    )
    out_specs = P(SP_TP, None)
    return jax.shard_map(body, mesh=split, in_specs=in_specs, out_specs=out_specs, check_vma=False)
```

time: 167 us -> 149 us (0.89)
  Pallas kernels: 163 us -> 147 us
    pallas_call x1, Pallas kernels: 163 us -> 147 us  [layer(): pl.pallas_call(layer_kernel, out_shape=jax.ShapeDtypeStruct((ROWS, MODEL)...]
where the time goes in v3:
time: 149 us
  Pallas kernels  147 us (99%)
  local copies, waits for them, and re-layouts  2.06 us (1%)
    pallas_call x1, Pallas kernels, layer(): pl.pallas_call(layer_kernel, out_shape=jax.ShapeDtypeStruct((ROWS, MODEL)...  147 us

profile of v3, /device:TPU:1, one launch (start us, length us, event | category | flops | bytes accessed | tf_op | source)
XLA Modules:
  0.0 149.1 jit_solution(3705440047878648911)
XLA Ops:
  0.0 147.0 %layer.1 = bf16[96,4096]{1,0:T(8,128)(2,1)} custom-call(bf16[96,4096]{1,0:T(8,128)(2,1)} %x_in.1, bf16[32,128]{1,0:T(8,128)(2,1)} %bitcast.4, bf16[256,256]{1,0:T(8,128)(2,1)} %w_q.1, bf16[256,256]{1,0:T(8,128)(2,1)} %w_k.1, bf16[256,512]{1,0:T(8,128)(2,1)} %w_v.1, bf16[256,512]{1,0:T(8,128)(2,1)} %w_out.1, bf16[256,512]{1,0:T(8,128)(2,1)} %w_in.1, ...), custom_call_target="tpu_custom_call" | custom-call | tf_op jit(solution)/shard_map/layer/pallas_call | solution.py:787
  147.0 2.1 %copy.18 = bf16[96,4096]{1,0:T(8,128)(2,1)} copy(bf16[96,4096]{1,0:T(8,128)(2,1)} %layer.1) | data formatting | bytes 1572864

commit v4 on v3

--- a/solution.py
+++ b/solution.py
@@ -67,105 +67,106 @@
 T_LAST = "last"
 ORDER = (
     (SEND, W, Q, 0, 0), (SEND, W, Q, 1, 4), (SEND, W, Q, 0, 1), (SEND, W, Q, 1, 5), (SEND, W, Q, 1, 0),
-    (SEND, W, Q, 0, 4), (SEND, W, Q, 1, 1), (SEND, W, Q, 0, 5), (RUN, T_NORM), (SEND, R, X, 0), (SEND, R, X, 2),
-    (SEND, R, X, 6), (SEND, W, E, 0, 0), (SEND, W, E, 0, 1), (SEND, W, E, 1, 0), (SEND, W, E, 1, 1),
-    (SEND, W, E, 0, 4), (SEND, W, E, 0, 5), (SEND, W, E, 1, 4), (SEND, W, E, 1, 5), (SEND, R, X, 1),
-    (SEND, R, X, 3), (WAIT, W, Q, 1, 0), (SEND, W, Q, 1, 6), (SEND, W, Q, 1, 7), (WAIT, W, Q, 0, 0),
-    (SEND, W, Q, 0, 6), (SEND, W, Q, 0, 7), (SEND, W, Q, 0, 2), (WAIT, W, Q, 0, 1), (SEND, W, Q, 0, 3),
-    (SEND, W, Q, 1, 2), (WAIT, W, Q, 1, 1), (SEND, W, Q, 1, 3), (SEND, W, Q, 0, 8), (SEND, W, Q, 0, 9),
-    (SEND, W, Q, 1, 8), (SEND, W, Q, 1, 9), (WAIT, R, X, 0), (SEND, R, X, 4), (WAIT, R, X, 2), (SEND, R, X, 5),
-    (WAIT, W, Q, 0, 4), (SEND, W, Q, 0, 12), (WAIT, W, Q, 0, 5), (SEND, W, Q, 0, 13), (WAIT, W, Q, 1, 4),
-    (SEND, W, Q, 1, 12), (WAIT, W, Q, 1, 5), (SEND, W, Q, 1, 13), (WAIT, W, Q, 0, 2), (WAIT, W, Q, 0, 3),
-    (SEND, W, Q, 0, 10), (SEND, W, Q, 0, 11), (WAIT, W, Q, 1, 2), (WAIT, W, Q, 1, 3), (SEND, W, Q, 1, 10),
-    (SEND, W, Q, 1, 11), (WAIT, R, X, 1), (SEND, R, X, 7), (WAIT, R, X, 3), (SEND, R, X, 8), (WAIT, W, Q, 0, 6),
-    (SEND, W, Q, 0, 14), (WAIT, W, Q, 0, 7), (SEND, W, Q, 0, 15), (WAIT, W, Q, 1, 6), (SEND, W, Q, 1, 14),
-    (WAIT, W, Q, 1, 7), (SEND, W, Q, 1, 15), (WAIT, W, E, 1, 0), (SEND, W, E, 1, 2), (WAIT, W, E, 1, 1),
-    (SEND, W, E, 1, 3), (WAIT, W, E, 0, 0), (SEND, W, E, 0, 2), (WAIT, W, E, 0, 1), (SEND, W, E, 0, 3),
-    (WAIT, W, Q, 0, 8), (SEND, W, Q, 0, 16), (WAIT, W, Q, 0, 9), (SEND, W, Q, 0, 17), (WAIT, W, Q, 1, 8),
-    (SEND, W, Q, 1, 16), (WAIT, W, Q, 1, 9), (SEND, W, Q, 1, 17), (SEND, W, E, 0, 6), (SEND, W, E, 0, 7),
-    (SEND, W, E, 1, 6), (SEND, W, E, 1, 7), (WAIT, R, X, 4), (WAIT, R, X, 5), (SEND, R, X, 9), (SEND, R, F, 6),
-    (SEND, R, F, 0), (SEND, R, F, 2), (WAIT, W, Q, 0, 10), (SEND, W, Q, 0, 18), (WAIT, W, Q, 0, 11),
-    (SEND, W, Q, 0, 19), (WAIT, W, Q, 1, 10), (SEND, W, Q, 1, 18), (WAIT, W, Q, 1, 11), (SEND, W, Q, 1, 19),
-    (WAIT, W, E, 0, 4), (SEND, W, E, 0, 12), (WAIT, W, E, 0, 5), (SEND, W, E, 0, 13), (WAIT, W, E, 1, 4),
-    (SEND, W, E, 1, 12), (WAIT, W, E, 1, 5), (SEND, W, E, 1, 13), (WAIT, W, Q, 0, 12), (WAIT, W, Q, 0, 13),
-    (WAIT, R, X, 6), (WAIT, R, X, 7), (WAIT, R, X, 8), (WAIT, R, X, 9), (RUN, T_PROJECT, Q, 0, 0),
-    (WAIT, W, E, 0, 2), (WAIT, W, E, 0, 3), (SEND, W, E, 0, 10), (SEND, W, E, 0, 11), (WAIT, W, E, 1, 2),
-    (WAIT, W, E, 1, 3), (SEND, W, E, 1, 10), (SEND, W, E, 1, 11), (WAIT, W, Q, 0, 14), (WAIT, W, Q, 0, 15),
-    (RUN, T_PROJECT, Q, 0, 1), (SEND, W, E, 0, 8), (SEND, W, E, 0, 9), (SEND, W, E, 1, 8), (SEND, W, E, 1, 9),
-    (WAIT, W, Q, 1, 12), (WAIT, W, Q, 1, 13), (RUN, T_PROJECT, Q, 1, 0), (WAIT, W, Q, 0, 16),
-    (WAIT, W, Q, 0, 17), (RUN, T_PROJECT, Q, 0, 2), (SEND, W, C, 0, 0), (SEND, W, C, 0, 1), (SEND, W, C, 1, 0),
-    (SEND, W, C, 1, 1), (WAIT, W, Q, 1, 14), (WAIT, W, Q, 1, 15), (RUN, T_PROJECT, Q, 1, 1), (SEND, R, F, 1),
-    (SEND, R, F, 3), (WAIT, W, Q, 1, 16), (WAIT, W, Q, 1, 17), (RUN, T_PROJECT, Q, 1, 2), (RUN, T_LOW_RANK),
-    (WAIT, W, E, 0, 6), (SEND, W, E, 0, 14), (SEND, W, C, 0, 4), (WAIT, W, E, 0, 7), (SEND, W, E, 0, 15),
-    (SEND, W, C, 0, 5), (WAIT, W, E, 1, 6), (SEND, W, E, 1, 14), (SEND, W, C, 1, 4), (WAIT, W, E, 1, 7),
-    (SEND, W, E, 1, 15), (SEND, W, C, 1, 5), (RUN, T_RATE, 0, 2), (RUN, T_RATE, 2, 4), (RUN, T_RATE, 4, 6),
-    (RUN, T_SUFFIX), (WAIT, W, E, 0, 10), (SEND, W, E, 0, 18), (WAIT, W, E, 0, 11), (SEND, W, E, 0, 19),
-    (WAIT, W, E, 1, 10), (SEND, W, E, 1, 18), (WAIT, W, E, 1, 11), (SEND, W, E, 1, 19), (WAIT, W, Q, 0, 18),
-    (WAIT, W, Q, 0, 19), (RUN, T_PROJECT, Q, 0, 3), (WAIT, W, E, 0, 8), (SEND, W, E, 0, 16), (WAIT, W, E, 0, 9),
-    (SEND, W, E, 0, 17), (WAIT, W, E, 1, 8), (SEND, W, E, 1, 16), (WAIT, W, E, 1, 9), (SEND, W, E, 1, 17),
-    (WAIT, W, Q, 1, 18), (WAIT, W, Q, 1, 19), (RUN, T_PROJECT, Q, 1, 3), (WAIT, W, C, 0, 0), (SEND, W, C, 0, 2),
-    (WAIT, W, C, 0, 1), (SEND, W, C, 0, 3), (WAIT, W, C, 1, 0), (SEND, W, C, 1, 2), (WAIT, W, C, 1, 1),
-    (SEND, W, C, 1, 3), (RUN, T_KEY_STATE), (WAIT, W, E, 0, 12), (WAIT, W, E, 0, 13), (RUN, T_PROJECT, E, 0, 0),
-    (SEND, S, 0, 0), (SEND, S, 0, 1), (SEND, W, C, 1, 6), (SEND, W, C, 1, 7), (WAIT, R, F, 0), (SEND, R, F, 4),
-    (WAIT, R, F, 2), (SEND, R, F, 5), (WAIT, W, E, 0, 14), (WAIT, W, E, 0, 15), (RUN, T_PROJECT, E, 0, 1),
-    (WAIT, W, E, 1, 12), (WAIT, W, E, 1, 13), (RUN, T_PROJECT, E, 1, 0), (WAIT, W, E, 1, 14),
-    (WAIT, W, E, 1, 15), (RUN, T_PROJECT, E, 1, 1), (SEND, W, C, 0, 6), (SEND, W, C, 0, 7), (SEND, W, C, 1, 8),
-    (SEND, W, C, 1, 9), (WAIT, W, E, 0, 16), (WAIT, W, E, 0, 17), (RUN, T_PROJECT, E, 0, 2),
-    (WAIT, W, E, 0, 18), (WAIT, W, E, 0, 19), (RUN, T_PROJECT, E, 0, 3), (WAIT, W, E, 1, 16),
-    (WAIT, W, E, 1, 17), (RUN, T_PROJECT, E, 1, 2), (WAIT, W, E, 1, 18), (WAIT, W, E, 1, 19),
-    (RUN, T_PROJECT, E, 1, 3), (WAIT, R, F, 1), (SEND, R, F, 7), (WAIT, R, F, 3), (SEND, R, F, 8),
-    (RUN, T_LOAD_H), (SEND, W, C, 0, 8), (SEND, W, C, 0, 9), (RUN, T_ATTEND, 0, 3), (RUN, T_ATTEND, 3, 6),
-    (WAIT, W, C, 1, 2), (WAIT, W, C, 1, 3), (SEND, W, C, 1, 10), (SEND, W, C, 1, 11), (RUN, T_ATTEND, 6, 9),
-    (RUN, T_START_H), (SEND, R, H, 6), (RUN, T_ATTEND, 9, 12), (SEND, R, H, 0), (SEND, R, H, 2),
-    (WAIT, S, 0, 0), (SEND, S, 0, 2), (WAIT, S, 0, 1), (SEND, S, 0, 3), (WAIT, W, C, 0, 2), (WAIT, W, C, 0, 3),
-    (SEND, W, C, 0, 10), (SEND, W, C, 0, 11), (WAIT, W, C, 1, 4), (SEND, W, C, 1, 12), (WAIT, W, C, 1, 5),
-    (SEND, W, C, 1, 13), (WAIT, W, C, 1, 8), (SEND, W, C, 1, 16), (WAIT, W, C, 1, 9), (SEND, W, C, 1, 17),
-    (WAIT, R, F, 4), (WAIT, R, F, 5), (SEND, R, F, 9), (WAIT, W, C, 0, 4), (SEND, W, C, 0, 12),
-    (WAIT, W, C, 0, 5), (SEND, W, C, 0, 13), (WAIT, W, C, 1, 6), (SEND, W, C, 1, 14), (WAIT, W, C, 1, 7),
-    (SEND, W, C, 1, 15), (WAIT, S, 0, 2), (WAIT, S, 0, 3), (RUN, T_FOLD_Y), (WAIT, W, C, 0, 8),
-    (SEND, W, C, 0, 16), (WAIT, W, C, 0, 9), (SEND, W, C, 0, 17), (SEND, S, 1, 0), (SEND, S, 1, 1),
-    (WAIT, W, C, 0, 6), (SEND, W, C, 0, 14), (WAIT, W, C, 0, 7), (SEND, W, C, 0, 15), (WAIT, W, C, 1, 12),
-    (WAIT, W, C, 1, 13), (RUN, T_PROJECT, C, 1, 0), (WAIT, W, C, 1, 10), (SEND, W, C, 1, 18),
-    (WAIT, W, C, 1, 11), (SEND, W, C, 1, 19), (SEND, R, H, 1), (SEND, R, H, 3), (WAIT, W, C, 0, 10),
-    (SEND, W, C, 0, 18), (WAIT, W, C, 0, 11), (SEND, W, C, 0, 19), (SEND, W, D, 0, 0), (SEND, W, D, 0, 1),
-    (SEND, W, D, 1, 0), (SEND, W, D, 1, 1), (WAIT, W, C, 1, 14), (WAIT, W, C, 1, 15), (RUN, T_PROJECT, C, 1, 1),
-    (WAIT, W, C, 0, 12), (WAIT, W, C, 0, 13), (RUN, T_PROJECT, C, 0, 0), (WAIT, W, C, 1, 16),
-    (WAIT, W, C, 1, 17), (RUN, T_PROJECT, C, 1, 2), (WAIT, S, 1, 0), (SEND, S, 1, 2), (WAIT, S, 1, 1),
-    (SEND, S, 1, 3), (SEND, W, D, 0, 4), (SEND, W, D, 0, 5), (SEND, W, D, 1, 4), (SEND, W, D, 1, 5),
-    (WAIT, W, C, 0, 14), (WAIT, W, C, 0, 15), (RUN, T_PROJECT, C, 0, 1), (WAIT, W, C, 0, 16),
-    (WAIT, W, C, 0, 17), (RUN, T_PROJECT, C, 0, 2), (WAIT, W, C, 1, 18), (WAIT, W, C, 1, 19),
-    (RUN, T_PROJECT, C, 1, 3), (WAIT, W, C, 0, 18), (WAIT, W, C, 0, 19), (RUN, T_PROJECT, C, 0, 3),
-    (RUN, T_GATE, C), (WAIT, R, H, 0), (SEND, R, H, 4), (WAIT, R, H, 2), (SEND, R, H, 5), (RUN, T_CONV, C),
-    (WAIT, W, D, 0, 0), (SEND, W, D, 0, 2), (WAIT, W, D, 0, 1), (SEND, W, D, 0, 3), (SEND, W, D, 0, 6),
-    (SEND, W, D, 0, 7), (WAIT, W, D, 1, 0), (SEND, W, D, 1, 6), (SEND, W, D, 1, 7), (WAIT, S, 1, 2),
-    (WAIT, S, 1, 3), (RUN, T_FOLD_Z), (RUN, T_FIRST_ROWS, C), (RUN, T_PAIR_PRODUCTS, 0),
-    (RUN, T_PAIR_PRODUCTS, 1), (SEND, W, D, 1, 2), (WAIT, W, D, 1, 1), (SEND, W, D, 1, 3),
-    (RUN, T_PAIR_PRODUCTS, 2), (RUN, T_PAIR_PRODUCTS, 3), (WAIT, R, H, 1), (SEND, R, H, 7), (WAIT, R, H, 3),
-    (SEND, R, H, 8), (RUN, T_FAR, 0), (RUN, T_FAR, 1), (WAIT, W, D, 0, 4), (SEND, W, D, 0, 12),
-    (WAIT, W, D, 0, 5), (SEND, W, D, 0, 13), (WAIT, W, D, 1, 4), (SEND, W, D, 1, 12), (WAIT, W, D, 1, 5),
-    (SEND, W, D, 1, 13), (RUN, T_FAR, 2), (RUN, T_FAR, 3), (WAIT, W, D, 0, 2), (WAIT, W, D, 0, 3),
-    (SEND, W, D, 0, 10), (SEND, W, D, 0, 11), (SEND, W, D, 1, 8), (SEND, W, D, 1, 9), (WAIT, W, D, 0, 6),
-    (SEND, W, D, 0, 14), (WAIT, W, D, 0, 7), (SEND, W, D, 0, 15), (WAIT, W, D, 1, 2), (WAIT, W, D, 1, 3),
-    (SEND, W, D, 1, 10), (SEND, W, D, 1, 11), (SEND, W, D, 0, 8), (SEND, W, D, 0, 9), (WAIT, W, D, 0, 12),
-    (WAIT, W, D, 0, 13), (RUN, T_PROJECT, D, 0, 0), (WAIT, W, D, 1, 12), (WAIT, W, D, 1, 13),
-    (RUN, T_PROJECT, D, 1, 0), (WAIT, R, H, 4), (WAIT, R, H, 5), (SEND, R, H, 9), (WAIT, W, D, 1, 6),
-    (SEND, W, D, 1, 14), (WAIT, W, D, 1, 7), (SEND, W, D, 1, 15), (RUN, T_NEAR, 0), (WAIT, W, D, 0, 10),
-    (SEND, W, D, 0, 18), (WAIT, W, D, 0, 11), (SEND, W, D, 0, 19), (WAIT, W, D, 1, 8), (SEND, W, D, 1, 16),
-    (WAIT, W, D, 1, 9), (SEND, W, D, 1, 17), (RUN, T_NEAR, 1), (RUN, T_NEAR, 2), (WAIT, W, D, 0, 14),
-    (WAIT, W, D, 0, 15), (RUN, T_PROJECT, D, 0, 1), (RUN, T_NEAR, 3), (WAIT, W, D, 1, 10), (SEND, W, D, 1, 18),
-    (WAIT, W, D, 1, 11), (SEND, W, D, 1, 19), (RUN, T_GATHER, 0), (RUN, T_PAIR_PRODUCTS, 4), (WAIT, W, D, 0, 8),
-    (SEND, W, D, 0, 16), (WAIT, W, D, 0, 9), (SEND, W, D, 0, 17), (WAIT, W, D, 1, 14), (WAIT, W, D, 1, 15),
-    (RUN, T_PROJECT, D, 1, 1), (RUN, T_GATHER, 1), (RUN, T_PAIR_PRODUCTS, 5), (RUN, T_FAR, 4),
-    (WAIT, W, D, 1, 16), (WAIT, W, D, 1, 17), (RUN, T_PROJECT, D, 1, 2), (RUN, T_GATHER, 2),
-    (RUN, T_PAIR_PRODUCTS, 6), (RUN, T_FAR, 5), (WAIT, W, D, 1, 18), (WAIT, W, D, 1, 19),
-    (RUN, T_PROJECT, D, 1, 3), (RUN, T_GATHER, 3), (RUN, T_PAIR_PRODUCTS, 7), (RUN, T_NEAR, 4),
-    (WAIT, W, D, 0, 16), (WAIT, W, D, 0, 17), (RUN, T_PROJECT, D, 0, 2), (WAIT, W, D, 0, 18),
-    (WAIT, W, D, 0, 19), (RUN, T_PROJECT, D, 0, 3), (RUN, T_NEAR, 5), (RUN, T_GATE, D), (RUN, T_CONV, D),
-    (RUN, T_FAR, 6), (RUN, T_FAR, 7), (RUN, T_GATHER, 4), (RUN, T_FIRST_ROWS, D), (RUN, T_EXCHANGE),
-    (RUN, T_GATHER, 5), (RUN, T_NEAR, 6), (RUN, T_NEAR, 7), (WAIT, R, F, 6), (WAIT, R, F, 7), (WAIT, R, F, 8),
-    (WAIT, R, F, 9), (WAIT, R, H, 6), (WAIT, R, H, 7), (WAIT, R, H, 8), (WAIT, R, H, 9), (RUN, T_COLLECT),
-    (RUN, T_LAST, 0), (RUN, T_LAST, 1), (RUN, T_LAST, 2), (RUN, T_LAST, 3), (RUN, T_LAST, 4),
-    (RUN, T_GATHER, 6), (RUN, T_LAST, 5), (RUN, T_LAST, 6), (RUN, T_GATHER, 7), (RUN, T_LAST, 7),
+    (SEND, W, Q, 0, 4), (SEND, W, Q, 1, 1), (SEND, W, Q, 0, 5), (SEND, R, F, 6), (RUN, T_NORM), (SEND, R, X, 0),
+    (SEND, R, X, 2), (SEND, R, X, 6), (SEND, W, E, 0, 0), (SEND, W, E, 0, 1), (SEND, W, E, 1, 0),
+    (SEND, W, E, 1, 1), (SEND, W, E, 0, 4), (SEND, W, E, 0, 5), (SEND, W, E, 1, 4), (SEND, W, E, 1, 5),
+    (SEND, R, X, 1), (SEND, R, X, 3), (WAIT, W, Q, 0, 0), (SEND, W, Q, 0, 2), (WAIT, W, Q, 0, 1),
+    (SEND, W, Q, 0, 3), (WAIT, W, Q, 1, 0), (SEND, W, Q, 1, 2), (WAIT, W, Q, 1, 1), (SEND, W, Q, 1, 3),
+    (SEND, W, Q, 0, 6), (SEND, W, Q, 0, 7), (SEND, W, Q, 1, 6), (SEND, W, Q, 1, 7), (SEND, W, Q, 0, 8),
+    (SEND, W, Q, 0, 9), (SEND, W, Q, 1, 8), (SEND, W, Q, 1, 9), (WAIT, R, X, 0), (SEND, R, X, 4),
+    (WAIT, R, X, 2), (SEND, R, X, 5), (WAIT, W, Q, 0, 2), (WAIT, W, Q, 0, 3), (SEND, W, Q, 0, 10),
+    (SEND, W, Q, 0, 11), (WAIT, W, Q, 1, 2), (WAIT, W, Q, 1, 3), (SEND, W, Q, 1, 10), (SEND, W, Q, 1, 11),
+    (WAIT, R, X, 1), (SEND, R, X, 7), (WAIT, R, X, 3), (SEND, R, X, 8), (WAIT, W, Q, 0, 6), (SEND, W, Q, 0, 14),
+    (WAIT, W, Q, 0, 7), (SEND, W, Q, 0, 15), (WAIT, W, Q, 1, 6), (SEND, W, Q, 1, 14), (WAIT, W, Q, 1, 7),
+    (SEND, W, Q, 1, 15), (SEND, R, F, 0), (SEND, R, F, 2), (WAIT, W, Q, 0, 8), (SEND, W, Q, 0, 16),
+    (WAIT, W, Q, 0, 9), (SEND, W, Q, 0, 17), (WAIT, W, Q, 1, 8), (SEND, W, Q, 1, 16), (WAIT, W, Q, 1, 9),
+    (SEND, W, Q, 1, 17), (WAIT, W, Q, 0, 4), (SEND, W, Q, 0, 12), (WAIT, W, Q, 0, 5), (SEND, W, Q, 0, 13),
+    (WAIT, W, Q, 1, 4), (SEND, W, Q, 1, 12), (WAIT, W, Q, 1, 5), (SEND, W, Q, 1, 13), (WAIT, W, Q, 0, 10),
+    (SEND, W, Q, 0, 18), (WAIT, W, Q, 0, 11), (SEND, W, Q, 0, 19), (WAIT, W, Q, 1, 10), (SEND, W, Q, 1, 18),
+    (WAIT, W, Q, 1, 11), (SEND, W, Q, 1, 19), (WAIT, R, X, 4), (WAIT, R, X, 5), (SEND, R, X, 9),
+    (WAIT, W, E, 0, 0), (SEND, W, E, 0, 2), (WAIT, W, E, 0, 1), (SEND, W, E, 0, 3), (WAIT, W, E, 1, 0),
+    (SEND, W, E, 1, 2), (WAIT, W, E, 1, 1), (SEND, W, E, 1, 3), (SEND, W, E, 0, 8), (SEND, W, E, 0, 9),
+    (SEND, W, E, 1, 8), (SEND, W, E, 1, 9), (SEND, W, E, 0, 6), (SEND, W, E, 0, 7), (SEND, W, E, 1, 6),
+    (SEND, W, E, 1, 7), (WAIT, W, E, 0, 4), (SEND, W, E, 0, 12), (WAIT, W, E, 0, 5), (SEND, W, E, 0, 13),
+    (WAIT, W, E, 1, 4), (SEND, W, E, 1, 12), (WAIT, W, E, 1, 5), (SEND, W, E, 1, 13), (WAIT, R, X, 6),
+    (WAIT, R, X, 7), (WAIT, R, X, 8), (WAIT, R, X, 9), (RUN, T_LOW_RANK), (SEND, W, C, 0, 0),
+    (SEND, W, C, 0, 1), (SEND, W, C, 1, 0), (SEND, W, C, 1, 1), (SEND, R, F, 1), (SEND, R, F, 3),
+    (RUN, T_RATE, 0, 2), (RUN, T_RATE, 2, 4), (RUN, T_RATE, 4, 6), (WAIT, W, E, 0, 2), (WAIT, W, E, 0, 3),
+    (SEND, W, E, 0, 10), (SEND, W, E, 0, 11), (WAIT, W, E, 1, 2), (WAIT, W, E, 1, 3), (SEND, W, E, 1, 10),
+    (SEND, W, E, 1, 11), (RUN, T_SUFFIX), (WAIT, W, Q, 0, 12), (WAIT, W, Q, 0, 13), (RUN, T_PROJECT, Q, 0, 0),
+    (WAIT, W, E, 0, 6), (SEND, W, E, 0, 14), (WAIT, W, E, 0, 8), (SEND, W, E, 0, 16), (WAIT, W, E, 0, 7),
+    (SEND, W, E, 0, 15), (WAIT, W, E, 0, 9), (SEND, W, E, 0, 17), (WAIT, W, E, 1, 6), (SEND, W, E, 1, 14),
+    (WAIT, W, E, 1, 8), (SEND, W, E, 1, 16), (WAIT, W, E, 1, 7), (SEND, W, E, 1, 15), (WAIT, W, E, 1, 9),
+    (SEND, W, E, 1, 17), (WAIT, W, Q, 0, 14), (WAIT, W, Q, 0, 15), (RUN, T_PROJECT, Q, 0, 1),
+    (SEND, W, C, 0, 4), (SEND, W, C, 0, 5), (SEND, W, C, 1, 4), (SEND, W, C, 1, 5), (WAIT, W, Q, 0, 16),
+    (WAIT, W, Q, 0, 17), (RUN, T_PROJECT, Q, 0, 2), (WAIT, W, Q, 0, 18), (WAIT, W, Q, 0, 19),
+    (RUN, T_PROJECT, Q, 0, 3), (WAIT, W, Q, 1, 12), (WAIT, W, Q, 1, 13), (RUN, T_PROJECT, Q, 1, 0),
+    (WAIT, W, Q, 1, 14), (WAIT, W, Q, 1, 15), (RUN, T_PROJECT, Q, 1, 1), (WAIT, W, Q, 1, 16),
+    (WAIT, W, Q, 1, 17), (RUN, T_PROJECT, Q, 1, 2), (WAIT, W, C, 0, 0), (SEND, W, C, 0, 2), (WAIT, W, C, 0, 1),
+    (SEND, W, C, 0, 3), (WAIT, W, C, 1, 0), (SEND, W, C, 1, 2), (WAIT, W, C, 1, 1), (SEND, W, C, 1, 3),
+    (WAIT, R, F, 0), (SEND, R, F, 4), (WAIT, R, F, 2), (SEND, R, F, 5), (WAIT, W, Q, 1, 18),
+    (WAIT, W, Q, 1, 19), (RUN, T_PROJECT, Q, 1, 3), (WAIT, W, E, 0, 10), (SEND, W, E, 0, 18),
+    (WAIT, W, E, 0, 11), (SEND, W, E, 0, 19), (WAIT, W, E, 1, 10), (SEND, W, E, 1, 18), (WAIT, W, E, 1, 11),
+    (SEND, W, E, 1, 19), (RUN, T_KEY_STATE), (SEND, S, 0, 0), (SEND, S, 0, 1), (SEND, W, C, 1, 6),
+    (SEND, W, C, 1, 7), (WAIT, W, E, 0, 12), (WAIT, W, E, 0, 13), (RUN, T_PROJECT, E, 0, 0),
+    (WAIT, W, E, 0, 14), (WAIT, W, E, 0, 15), (RUN, T_PROJECT, E, 0, 1), (WAIT, W, E, 0, 16),
+    (WAIT, W, E, 0, 17), (RUN, T_PROJECT, E, 0, 2), (WAIT, W, E, 1, 12), (WAIT, W, E, 1, 13),
+    (RUN, T_PROJECT, E, 1, 0), (WAIT, W, E, 1, 14), (WAIT, W, E, 1, 15), (RUN, T_PROJECT, E, 1, 1),
+    (SEND, W, C, 0, 6), (SEND, W, C, 0, 7), (WAIT, W, E, 1, 16), (WAIT, W, E, 1, 17), (RUN, T_PROJECT, E, 1, 2),
+    (WAIT, R, F, 1), (SEND, R, F, 7), (WAIT, R, F, 3), (SEND, R, F, 8), (WAIT, W, C, 1, 4), (SEND, W, C, 1, 12),
+    (WAIT, W, C, 1, 5), (SEND, W, C, 1, 13), (WAIT, W, C, 1, 2), (WAIT, W, C, 1, 3), (SEND, W, C, 1, 10),
+    (SEND, W, C, 1, 11), (WAIT, W, E, 0, 18), (WAIT, W, E, 0, 19), (RUN, T_PROJECT, E, 0, 3),
+    (WAIT, W, C, 0, 2), (WAIT, W, C, 0, 3), (SEND, W, C, 0, 10), (SEND, W, C, 0, 11), (WAIT, W, E, 1, 18),
+    (WAIT, W, E, 1, 19), (RUN, T_PROJECT, E, 1, 3), (RUN, T_LOAD_H), (RUN, T_ATTEND, 0, 3),
+    (RUN, T_ATTEND, 3, 6), (RUN, T_ATTEND, 6, 9), (RUN, T_START_H), (SEND, R, H, 6), (WAIT, S, 0, 0),
+    (SEND, S, 0, 2), (WAIT, S, 0, 1), (SEND, S, 0, 3), (WAIT, W, C, 1, 6), (SEND, W, C, 1, 14),
+    (WAIT, W, C, 1, 7), (SEND, W, C, 1, 15), (SEND, R, H, 0), (SEND, R, H, 2), (RUN, T_ATTEND, 9, 12),
+    (WAIT, W, C, 0, 4), (SEND, W, C, 0, 12), (WAIT, W, C, 0, 5), (SEND, W, C, 0, 13), (SEND, W, C, 1, 8),
+    (SEND, W, C, 1, 9), (WAIT, W, C, 1, 12), (WAIT, W, C, 1, 13), (RUN, T_PROJECT, C, 1, 0), (WAIT, W, C, 0, 6),
+    (SEND, W, C, 0, 14), (WAIT, W, C, 0, 7), (SEND, W, C, 0, 15), (WAIT, R, F, 4), (WAIT, R, F, 5),
+    (SEND, R, F, 9), (SEND, W, C, 0, 8), (SEND, W, C, 0, 9), (WAIT, W, C, 1, 10), (SEND, W, C, 1, 18),
+    (WAIT, W, C, 1, 11), (SEND, W, C, 1, 19), (SEND, W, D, 1, 4), (SEND, W, D, 1, 5), (WAIT, W, C, 1, 14),
+    (WAIT, W, C, 1, 15), (RUN, T_PROJECT, C, 1, 1), (SEND, R, H, 1), (SEND, R, H, 3), (WAIT, S, 0, 2),
+    (WAIT, S, 0, 3), (RUN, T_FOLD_Y), (WAIT, W, C, 0, 10), (SEND, W, C, 0, 18), (WAIT, W, C, 0, 11),
+    (SEND, W, C, 0, 19), (WAIT, W, C, 0, 12), (WAIT, W, C, 0, 13), (RUN, T_PROJECT, C, 0, 0), (SEND, S, 1, 0),
+    (SEND, S, 1, 1), (SEND, W, D, 0, 4), (SEND, W, D, 0, 5), (WAIT, W, C, 0, 14), (WAIT, W, C, 0, 15),
+    (RUN, T_PROJECT, C, 0, 1), (WAIT, W, C, 1, 8), (SEND, W, C, 1, 16), (WAIT, W, C, 1, 9), (SEND, W, C, 1, 17),
+    (WAIT, W, C, 0, 8), (SEND, W, C, 0, 16), (WAIT, W, C, 0, 9), (SEND, W, C, 0, 17), (SEND, W, D, 0, 0),
+    (SEND, W, D, 0, 1), (SEND, W, D, 1, 0), (SEND, W, D, 1, 1), (WAIT, R, H, 0), (SEND, R, H, 4),
+    (WAIT, R, H, 2), (SEND, R, H, 5), (WAIT, S, 1, 0), (SEND, S, 1, 2), (WAIT, S, 1, 1), (SEND, S, 1, 3),
+    (WAIT, W, D, 0, 4), (SEND, W, D, 0, 12), (WAIT, W, D, 0, 5), (SEND, W, D, 0, 13), (WAIT, W, D, 1, 4),
+    (SEND, W, D, 1, 12), (WAIT, W, D, 1, 5), (SEND, W, D, 1, 13), (WAIT, W, C, 1, 16), (WAIT, W, C, 1, 17),
+    (RUN, T_PROJECT, C, 1, 2), (WAIT, W, C, 1, 18), (WAIT, W, C, 1, 19), (RUN, T_PROJECT, C, 1, 3),
+    (WAIT, W, C, 0, 16), (WAIT, W, C, 0, 17), (RUN, T_PROJECT, C, 0, 2), (WAIT, W, C, 0, 18),
+    (WAIT, W, C, 0, 19), (RUN, T_PROJECT, C, 0, 3), (WAIT, R, H, 1), (SEND, R, H, 7), (WAIT, R, H, 3),
+    (SEND, R, H, 8), (RUN, T_GATE, C), (RUN, T_CONV, C), (WAIT, W, D, 0, 0), (SEND, W, D, 0, 2),
+    (WAIT, W, D, 0, 1), (SEND, W, D, 0, 3), (SEND, W, D, 0, 6), (SEND, W, D, 0, 7), (WAIT, W, D, 1, 0),
+    (SEND, W, D, 1, 6), (SEND, W, D, 1, 7), (SEND, W, D, 1, 2), (WAIT, W, D, 1, 1), (SEND, W, D, 1, 3),
+    (WAIT, S, 1, 2), (WAIT, S, 1, 3), (RUN, T_FOLD_Z), (RUN, T_FIRST_ROWS, C), (RUN, T_PAIR_PRODUCTS, 0),
+    (SEND, W, D, 0, 8), (SEND, W, D, 0, 9), (SEND, W, D, 1, 8), (SEND, W, D, 1, 9), (RUN, T_PAIR_PRODUCTS, 1),
+    (RUN, T_PAIR_PRODUCTS, 2), (RUN, T_PAIR_PRODUCTS, 3), (RUN, T_FAR, 0), (WAIT, W, D, 0, 12),
+    (WAIT, W, D, 0, 13), (RUN, T_PROJECT, D, 0, 0), (RUN, T_FAR, 1), (WAIT, W, D, 1, 12), (WAIT, W, D, 1, 13),
+    (RUN, T_PROJECT, D, 1, 0), (RUN, T_FAR, 2), (WAIT, W, D, 0, 6), (SEND, W, D, 0, 14), (WAIT, W, D, 0, 7),
+    (SEND, W, D, 0, 15), (RUN, T_FAR, 3), (WAIT, W, D, 1, 6), (SEND, W, D, 1, 14), (WAIT, W, D, 1, 7),
+    (SEND, W, D, 1, 15), (WAIT, W, D, 0, 2), (WAIT, W, D, 0, 3), (SEND, W, D, 0, 10), (SEND, W, D, 0, 11),
+    (WAIT, W, D, 1, 2), (WAIT, W, D, 1, 3), (SEND, W, D, 1, 10), (SEND, W, D, 1, 11), (WAIT, R, H, 4),
+    (WAIT, R, H, 5), (SEND, R, H, 9), (RUN, T_NEAR, 0), (RUN, T_NEAR, 1), (RUN, T_NEAR, 2), (WAIT, W, D, 0, 8),
+    (SEND, W, D, 0, 16), (WAIT, W, D, 0, 9), (SEND, W, D, 0, 17), (WAIT, W, D, 1, 8), (SEND, W, D, 1, 16),
+    (WAIT, W, D, 1, 9), (SEND, W, D, 1, 17), (RUN, T_NEAR, 3), (WAIT, W, D, 0, 14), (WAIT, W, D, 0, 15),
+    (RUN, T_PROJECT, D, 0, 1), (RUN, T_GATHER, 0), (RUN, T_PAIR_PRODUCTS, 4), (WAIT, W, D, 1, 14),
+    (WAIT, W, D, 1, 15), (RUN, T_PROJECT, D, 1, 1), (RUN, T_GATHER, 1), (RUN, T_PAIR_PRODUCTS, 5),
+    (RUN, T_FAR, 4), (WAIT, W, D, 0, 10), (SEND, W, D, 0, 18), (WAIT, W, D, 0, 11), (SEND, W, D, 0, 19),
+    (WAIT, W, D, 1, 10), (SEND, W, D, 1, 18), (WAIT, W, D, 1, 11), (SEND, W, D, 1, 19), (RUN, T_GATHER, 2),
+    (RUN, T_PAIR_PRODUCTS, 6), (RUN, T_FAR, 5), (WAIT, W, D, 0, 16), (WAIT, W, D, 0, 17),
+    (RUN, T_PROJECT, D, 0, 2), (RUN, T_GATHER, 3), (RUN, T_FAR, 6), (RUN, T_PAIR_PRODUCTS, 7), (RUN, T_NEAR, 4),
+    (WAIT, W, D, 1, 16), (WAIT, W, D, 1, 17), (RUN, T_PROJECT, D, 1, 2), (RUN, T_NEAR, 5), (WAIT, W, D, 0, 18),
+    (WAIT, W, D, 0, 19), (RUN, T_PROJECT, D, 0, 3), (RUN, T_FAR, 7), (WAIT, W, D, 1, 18), (WAIT, W, D, 1, 19),
+    (RUN, T_PROJECT, D, 1, 3), (RUN, T_GATE, D), (RUN, T_NEAR, 6), (RUN, T_CONV, D), (RUN, T_GATHER, 4),
+    (RUN, T_FIRST_ROWS, D), (RUN, T_EXCHANGE), (RUN, T_GATHER, 5), (RUN, T_NEAR, 7), (RUN, T_GATHER, 6),
+    (WAIT, R, F, 6), (WAIT, R, F, 7), (WAIT, R, F, 8), (WAIT, R, F, 9), (WAIT, R, H, 6), (WAIT, R, H, 7),
+    (WAIT, R, H, 8), (WAIT, R, H, 9), (RUN, T_COLLECT), (RUN, T_LAST, 0), (RUN, T_LAST, 1), (RUN, T_LAST, 2),
+    (RUN, T_LAST, 3), (RUN, T_LAST, 4), (RUN, T_GATHER, 7), (RUN, T_LAST, 5), (RUN, T_LAST, 6),
+    (RUN, T_LAST, 7),
 )
 
 
@@ -309,7 +310,7 @@
             pltpu.make_async_copy(
                 w_c.at[EARLY + 128 : 512, pl.ds(i * 512, 512)],
                 qab.at[pl.ds(pl.multiple_of(t * 1024 + i * 128, 128), 128), :],
-                load_sem.at[14 + i],
+                load_sem.at[15 + i],
             )
             for i in range(8)
         ]
@@ -321,8 +322,6 @@
             pltpu.make_async_copy(w_c.at[0:EARLY, cols], wo.at[i % 3, 512:MIX, :], out_sem.at[2 * i + 1]),
         )
 
-    for c in loads[1:]:
-        c.wait()
     pl.semaphore_wait(barrier, len(peers))
 
     started = []
@@ -416,6 +415,8 @@
             return w_copy(g, p, slot, k, 1 if side else 3, 1, step)
         return w_copy(g, p, slot, k, 2, 1, step, row, 128)
 
+    waiting = {"q": (1, 2, 4), "e": (3, 5), "c": (6, 7, 8, 9), "d": (10, 11, 12, 13), "f": (14,)}
+
     ring_sent = (
         (0, True, 1, 1), (0, False, 1, 1), (0, False, 1, 3), (0, True, 1, 3), (3, True, 1, 1), (1, False, 1, 3),
         (0, True, 2, 0), (3, True, 2, 0), (1, True, 2, 0), (2, True, 2, 0),
@@ -436,6 +437,8 @@
 
     class Device:
         def send(self, kind, *a):
+            for i in waiting.pop(a[0], ()):
+                loads[i].wait()
             if kind == "w":
                 go(w_sent(*a), a[0])
             elif kind == "r":
@@ -786,7 +789,7 @@
 
     return pl.pallas_call(
         layer_kernel,
-        out_shape=jax.ShapeDtypeStruct((ROWS, MODEL), BF16),
+        out_shape=pltpu.VMEM((ROWS, MODEL), BF16),
         in_specs=[any_, vmem] + [any_] * 6 + [vmem] * 6 + [any_] * 2,
         out_specs=vmem,
         scratch_shapes=[
@@ -826,7 +829,7 @@
             bf16(CHUNKS, 2, 48, CW),
             bf16(4, 2, ROWS, CW),
             bf16(CHUNKS, 2, ROWS, CW),
-            dma((22,)),
+            dma((23,)),
             dma((2 * CHUNKS,)),
             dma((8, 20)),
             dma((8, 20)),
@@ -847,7 +850,7 @@
             pltpu.SemaphoreType.REGULAR,
         ],
         compiler_params=pltpu.CompilerParams(
-            collective_id=0, has_side_effects=True, vmem_limit_bytes=67_000_000
+            collective_id=0, has_side_effects=True, vmem_limit_bytes=66_100_000
         ),
         name="layer",
     )(*args)

time: 149 us -> 146 us (0.980)
  Pallas kernels: 147 us -> 145 us
    pallas_call x1, Pallas kernels: 147 us -> 145 us  [layer(): pl.pallas_call(layer_kernel, out_shape=pltpu.VMEM((ROWS, MODEL), BF16), i...]
where the time goes in v4:
time: 146 us
  Pallas kernels  145 us (99%)
    pallas_call x1, Pallas kernels, layer(): pl.pallas_call(layer_kernel, out_shape=pltpu.VMEM((ROWS, MODEL), BF16), i...  145 us

profile of v4, /device:TPU:1, one launch (start us, length us, event | category | flops | bytes accessed | tf_op | source)
XLA Modules:
  0.0 146.3 jit_solution(12103921245900211178)
XLA Ops:
  0.0 145.4 %layer.1 = bf16[96,4096]{1,0:T(8,128)(2,1)S(1)} custom-call(bf16[96,4096]{1,0:T(8,128)(2,1)} %x_in.1, bf16[32,128]{1,0:T(8,128)(2,1)} %bitcast.4, bf16[256,256]{1,0:T(8,128)(2,1)} %w_q.1, bf16[256,256]{1,0:T(8,128)(2,1)} %w_k.1, bf16[256,512]{1,0:T(8,128)(2,1)} %w_v.1, bf16[256,512]{1,0:T(8,128)(2,1)} %w_out.1, bf16[256,512]{1,0:T(8,128)(2,1)} %w_in.1, ...), custom_call_target="tpu_custom_call" | custom-call | tf_op jit(solution)/shard_map/layer/pallas_call | solution.py:790
  145.4 0.9 copy.18
